TPU v7x, 128 devices: a whole 4x4x4 slice. The times are simulated.
128 devices in a mesh: sp: 32 (over z, y, core), tp: 4 (over x).
Axes of the slice: x: 4, y: 4, z: 4, core: 2. Of those that a mesh axis runs over, the one named last changes fastest.
Arguments:
- tokens: bfloat16 [12288, 4096], P(('sp', 'tp')), may hold values from -6 to 6
- norm_gain: float32 [4096], replicated, may hold values from 0.1 to 1.9
- w_query: bfloat16 [4096, 2048], P('sp', 'tp'), may hold values from -0.09375 to 0.09375
- w_key: bfloat16 [4096, 512], P('sp', 'tp'), may hold values from -1.5 to 1.5
- w_value: bfloat16 [4096, 512], P('sp', 'tp'), may hold values from -0.09375 to 0.09375
- w_mem_query: bfloat16 [4096, 1024], P('sp', 'tp'), may hold values from -0.09375 to 0.09375
- w_mem_key: bfloat16 [4096, 1024], P('sp', 'tp'), may hold values from -0.09375 to 0.09375
- w_mem_value: bfloat16 [4096, 1024], P('sp', 'tp'), may hold values from -0.09375 to 0.09375
- w_mem_gate: bfloat16 [4096, 1024], P('sp', 'tp'), may hold values from -0.09375 to 0.09375
- w_gates: bfloat16 [4096, 2, 16], replicated, may hold values from -0.09375 to 0.09375
- sinks: float32 [32], P('tp'), may hold values from 2 to 6
- forget_bias: float32 [16], P('tp'), may hold values from 3 to 13
- forget_shift: float32 [12288, 16], P('sp', 'tp'), may hold values from -1 to 0
- w_out: bfloat16 [3072, 4096], P('sp', 'tp'), may hold values from -0.21650635 to 0.21650635
Outputs:
- mixed: bfloat16 [12288, 4096], P('sp', 'tp')
- log_total: float32 [12288, 32], P('sp', 'tp')
All inputs are finite; a program needn't handle non-finite values.
Results may differ from a plain program's by a relative error of at most 0.018.
Values may be sent and summed in bfloat16 or wider, within the bound.
A program may use at most 128 MiB of HBM per device.

v0:
```python
import math

import jax
import jax.numpy as jnp
from jax import lax
from jax.sharding import Mesh
from jax.sharding import PartitionSpec as P

HD = 64
WINDOW = 128
BLK = 128
SP = ("sp_0", "sp_1", "sp_2")
SP_TP = ("sp_0", "sp_1", "sp_2", "tp")


EPSILON = 1e-06
MASKED = -1e30
exact_precision = lax.Precision.HIGHEST


def passed_along(block, axis, distance):
    devices = range(lax.axis_size(axis))
    route = [(i - distance, i) for i in devices if i - distance in devices]
    return lax.ppermute(block, axis, route)


def nothing_yet(x, identity):
    return jax.tree.map(
        lambda a, e: jnp.broadcast_to(jnp.asarray(e, a.dtype), a.shape), x, identity
    )


def collected_together(x, axis):
    leaves = jax.tree.leaves(x)
    turns = sorted(range(len(leaves)), key=lambda k: -leaves[k].size)
    width = (1, *leaves[turns[0]].shape)[-1]
    lines = [
        jnp.pad(leaves[k].reshape(-1), (0, -leaves[k].size % width)).reshape(-1, width)
        for k in turns
    ]
    both, at, found = (lax.all_gather(jnp.concatenate(lines), axis), 0, {})
    for k, line in zip(turns, lines):
        section = both[:, at : at + len(line)].reshape(len(both), -1)
        found[k] = section[:, : leaves[k].size].reshape(-1, *leaves[k].shape)
        at += len(line)
    numbers = iter(range(len(leaves)))
    return jax.tree.map(lambda _: found[next(numbers)], x)


def entering(x, axes, combine, identity):
    before = start = nothing_yet(x, identity)
    total = x
    for axis in reversed(axes):
        length, mine = (lax.axis_size(axis), lax.axis_index(axis))
        pieces = collected_together(
            jax.tree.map(
                lambda part, kind: part.astype(kind),
                total,
                (jnp.bfloat16, jnp.bfloat16, jnp.bfloat16, jnp.bfloat16),
            ),
            axis,
        )
        inside, total = (start, start)
        for k in range(length):
            passed = k < mine
            total = combine(
                total, jax.tree.map(lambda part, own: part[k].astype(own.dtype), pieces, x)
            )
            inside = jax.tree.map(lambda new, old: jnp.where(passed, new, old), total, inside)
        before = combine(inside, before)
    return before


def from_everyone(x, axis):
    copies = jnp.broadcast_to(x, (lax.axis_size(axis), *x.shape))
    return lax.all_to_all(copies, axis, split_axis=0, concat_axis=0, tiled=True)


def joined_along(pieces, dim):
    pieces = jnp.moveaxis(pieces, 0, dim)
    shape = pieces.shape
    return pieces.reshape(*shape[:dim], shape[dim] * shape[dim + 1], *shape[dim + 2 :])


def gather_directly(x, axis, dim):
    pieces = from_everyone(x, axis)
    return joined_along(pieces, dim)


def in_one_piece(arrays, axis, dim, along):
    ends, at = ([], 0)
    for a in arrays[:-1]:
        at += a.shape[along]
        ends.append(at)
    both = jnp.concatenate(arrays, axis=along)
    return tuple(jnp.split(lax.all_gather(both, axis, axis=dim, tiled=True), ends, axis=along))


def normalize(tokens, norm_gain):
    values = tokens.astype(jnp.float32)
    rescale = lax.rsqrt(jnp.mean(values * values, axis=-1, keepdims=True) + EPSILON)
    return (values * rescale * norm_gain).astype(jnp.bfloat16)


def advance(carried, key_block, value_block, in_block, cumulative):
    memory_state, normalizer, stabilizer = carried
    block_total = cumulative[:, -1]
    decays = block_total[:, None] - cumulative + in_block
    new_stabilizer = jnp.maximum(block_total + stabilizer, jnp.max(decays, axis=-1))
    weights = jnp.exp(decays - new_stabilizer[:, None])
    rescale = jnp.exp(block_total + stabilizer - new_stabilizer)
    new_state = rescale[:, None, None] * memory_state + jnp.einsum(
        "hsv,hsk->hvk", value_block * weights[:, :, None], key_block, precision=exact_precision
    )
    new_normalizer = rescale[:, None] * normalizer + jnp.einsum(
        "hs,hsk->hk", weights, key_block, precision=exact_precision
    )
    return (new_state, new_normalizer, new_stabilizer)


def block_step(carried, block_data):
    memory_state, normalizer, stabilizer = carried
    query_block, key_block, value_block, in_block, forget_block = block_data
    length = in_block.shape[-1]
    cumulative = jnp.cumsum(forget_block, axis=-1)
    causal = lax.broadcasted_iota(jnp.int32, (length, length), 0) >= lax.broadcasted_iota(
        jnp.int32, (length, length), 1
    )
    log_weight = jnp.where(
        causal[None], cumulative[:, :, None] - cumulative[:, None, :] + in_block[:, None, :], MASKED
    )
    row_level = jnp.maximum(cumulative + stabilizer[:, None], jnp.max(log_weight, axis=-1))
    carried_part = jnp.exp(cumulative + stabilizer[:, None] - row_level)
    affinity = jnp.einsum(
        "htd,hsd->hts", query_block, key_block, precision=exact_precision
    ) * jnp.exp(log_weight - row_level[:, :, None])
    numerator = carried_part[:, :, None] * jnp.einsum(
        "hvk,htk->htv", memory_state, query_block, precision=exact_precision
    ) + jnp.einsum("hts,hsv->htv", affinity, value_block, precision=exact_precision)
    denominator = carried_part * jnp.einsum(
        "hk,htk->ht", normalizer, query_block, precision=exact_precision
    ) + jnp.sum(affinity, axis=-1)
    recall = numerator / jnp.maximum(jnp.abs(denominator), jnp.exp(-row_level))[:, :, None]
    return (advance(carried, key_block, value_block, in_block, cumulative), recall)


def join_states(earlier, later):
    passed_one, state_one, normal_one, level_one = earlier
    passed_two, state_two, normal_two, level_two = later
    new_level = jnp.maximum(passed_two + level_one, level_two)
    weight_one = jnp.exp(passed_two + level_one - new_level)
    weight_two = jnp.exp(level_two - new_level)
    new_state = weight_one[:, None, None] * state_one + weight_two[:, None, None] * state_two
    new_normal = weight_one[:, None] * normal_one + weight_two[:, None] * normal_two
    return (passed_one + passed_two, new_state, new_normal, new_level)


def attend(query, key_rows, value_rows, sinks):
    row_count = query.shape[0]
    kv_local = key_rows.shape[1] // HD
    group_size = query.shape[1] // HD // kv_local
    block_count = row_count // WINDOW
    rim_key, rim_value = passed_along(
        (key_rows[row_count - WINDOW :], value_rows[row_count - WINDOW :]), SP, 1
    )
    padded_keys = jnp.concatenate([rim_key, key_rows], axis=0).reshape(
        block_count + 1, WINDOW, kv_local, HD
    )
    padded_values = jnp.concatenate([rim_value, value_rows], axis=0).reshape(
        block_count + 1, WINDOW, kv_local, HD
    )
    key_window = jnp.concatenate([padded_keys[:-1], padded_keys[1:]], axis=1)
    value_window = jnp.concatenate([padded_values[:-1], padded_values[1:]], axis=1)
    q_blocks = query.reshape(block_count, WINDOW, kv_local, group_size, HD)
    scores = jnp.einsum(
        "nqhgd,nkhd->nhgqk", q_blocks, key_window, preferred_element_type=jnp.float32
    ) * HD ** (-0.5)
    query_index = lax.broadcasted_iota(jnp.int32, (WINDOW, 2 * WINDOW), 0)
    key_index = lax.broadcasted_iota(jnp.int32, (WINDOW, 2 * WINDOW), 1)
    distance = query_index - key_index + WINDOW
    in_band = (distance >= 0) & (distance < WINDOW)
    block_index = lax.broadcasted_iota(jnp.int32, (block_count, WINDOW, 2 * WINDOW), 0)
    key_position = lax.axis_index(SP) * row_count + block_index * WINDOW - WINDOW + key_index[None]
    allowed = (in_band[None] & (key_position >= 0))[:, None, None]
    scores = jnp.where(allowed, scores, MASKED)
    sink_logit = sinks.reshape(1, kv_local, group_size, 1, 1)
    ceiling = jnp.maximum(jnp.max(scores, axis=-1, keepdims=True), sink_logit)
    weights = jnp.exp(scores - ceiling)
    partition = jnp.exp(sink_logit - ceiling) + jnp.sum(weights, axis=-1, keepdims=True)
    log_total = (
        (ceiling + jnp.log(partition))[..., 0]
        .transpose(0, 3, 1, 2)
        .reshape(row_count, kv_local * group_size)
    )
    probs = (weights / partition).astype(jnp.bfloat16)
    head_out = jnp.einsum(
        "nhgqk,nkhd->nqhgd", probs, value_window, preferred_element_type=jnp.float32
    )
    return (head_out.astype(jnp.bfloat16).reshape(row_count, kv_local * group_size * HD), log_total)


def memory(mem_query, mem_key, mem_value, mem_gate, gate_pre, forget_bias, forget_shift):
    row_count = mem_query.shape[0]
    head_count = forget_bias.shape[0]
    block_count = row_count // BLK
    sequence_total = row_count * lax.axis_size(SP)

    def blocks(array):
        return (
            array.astype(jnp.float32)
            .reshape(block_count, BLK, head_count, HD)
            .transpose(0, 2, 1, 3)
        )

    def gate_blocks(array):
        return array.reshape(block_count, BLK, head_count).transpose(0, 2, 1)

    log_in = gate_pre[:, 0, :] - 0.5 * math.log(sequence_total)
    log_forget = jax.nn.log_sigmoid(gate_pre[:, 1, :] + forget_bias) + forget_shift
    query_blocks = blocks(mem_query)
    key_blocks = blocks(mem_key) * HD ** (-0.5)
    value_blocks = blocks(mem_value)
    in_blocks = gate_blocks(log_in)
    forget_blocks = gate_blocks(log_forget)
    initial = (
        jnp.zeros((head_count, HD, HD), jnp.float32),
        jnp.zeros((head_count, HD), jnp.float32),
        jnp.full((head_count,), MASKED, jnp.float32),
    )

    def summarize(carried, block_data):
        key_block, value_block, in_block, forget_block = block_data
        return (
            advance(carried, key_block, value_block, in_block, jnp.cumsum(forget_block, axis=-1)),
            None,
        )

    summary, _ = lax.scan(summarize, initial, (key_blocks, value_blocks, in_blocks, forget_blocks))
    passed = jnp.sum(log_forget, axis=0)
    identity = (jnp.zeros((head_count,), jnp.float32), initial[0], initial[1], initial[2])
    incoming = entering((passed, summary[0], summary[1], summary[2]), SP, join_states, identity)
    _, recall = lax.scan(
        block_step,
        (incoming[1], incoming[2], incoming[3]),
        (query_blocks, key_blocks, value_blocks, in_blocks, forget_blocks),
    )
    recall = recall.transpose(0, 2, 1, 3).reshape(row_count, head_count * HD)
    return (recall * jax.nn.sigmoid(mem_gate.astype(jnp.float32))).astype(jnp.bfloat16)


def shards(
    tokens,
    norm_gain,
    w_query,
    w_key,
    w_value,
    w_mem_query,
    w_mem_key,
    w_mem_value,
    w_mem_gate,
    w_gates,
    sinks,
    forget_bias,
    forget_shift,
    w_out,
):
    normed = normalize(tokens, norm_gain)
    out_whole = lax.all_gather(w_out, SP, axis=0, tiled=True)
    token_rows = gather_directly(normed, "tp", 0)
    row_count = token_rows.shape[0]
    head_count = forget_bias.shape[0]
    gate_columns = lax.dynamic_slice_in_dim(
        w_gates, lax.axis_index("tp") * head_count, head_count, 2
    ).reshape(w_gates.shape[0], 2 * head_count)
    gate_pre = jnp.dot(token_rows, gate_columns, preferred_element_type=jnp.float32).reshape(
        row_count, 2, head_count
    )

    def add_pieces(segments):
        return tuple(
            (
                jnp.dot(token_rows, segment, preferred_element_type=jnp.float32)
                for segment in segments
            )
        )

    attn_sums = add_pieces(in_one_piece((w_query, w_key, w_value), SP, 0, 1))
    attn_parts = [partial_sum.astype(jnp.bfloat16) for partial_sum in attn_sums]
    attn_out, log_total = attend(attn_parts[0], attn_parts[1], attn_parts[2], sinks)
    mem_sums = add_pieces(in_one_piece((w_mem_query, w_mem_key, w_mem_value, w_mem_gate), SP, 0, 1))
    mem_parts = [partial_sum.astype(jnp.bfloat16) for partial_sum in mem_sums]
    mem_out = memory(
        mem_parts[0], mem_parts[1], mem_parts[2], mem_parts[3], gate_pre, forget_bias, forget_shift
    )
    head_attn, head_mem = (gather_directly(attn_out, "tp", 1), gather_directly(mem_out, "tp", 1))
    joined = jnp.concatenate([head_attn, head_mem], axis=1)
    mixed = jnp.dot(joined, out_whole, preferred_element_type=jnp.float32)
    return (mixed.astype(jnp.bfloat16), log_total)


def solution(mesh):
    torus = Mesh(mesh.devices.reshape(4, 4, 2, mesh.shape["tp"]), ("sp_0", "sp_1", "sp_2", "tp"))
    placed = (
        P(SP_TP, None),
        P(),
        P(SP, "tp"),
        P(SP, "tp"),
        P(SP, "tp"),
        P(SP, "tp"),
        P(SP, "tp"),
        P(SP, "tp"),
        P(SP, "tp"),
        P(),
        P("tp"),
        P("tp"),
        P(SP, "tp"),
        P(SP, "tp"),
    )
    return jax.shard_map(
        shards, mesh=torus, in_specs=placed, out_specs=(P(SP, "tp"), P(SP, "tp")), check_vma=False
    )
```

profile of v0, /device:TPU:0, one launch (start us, length us, event | category | flops | bytes accessed | tf_op | source)
XLA Modules:
  0.0 221.4 jit_solution(14271454618328555398)
XLA Ops:
  7.2 1.7 pad_maximum_fusion.1
  9.0 1.7 pad_maximum_fusion
  10.7 1.4 fusion.49
  12.1 1.4 fusion.51
  13.5 2.1 broadcast_in_dim.41
  15.6 4.8 %all-to-all-start = ((bf16[4,96,4096]{2,1,0:T(8,128)(2,1)}), bf16[4,96,4096]{2,1,0:T(8,128)(2,1)}, u32[]{:S(2)}, u32[]{:S(2)}) async-start(bf16[4,96,4096]{2,1,0:T(8,128)(2,1)} %broadcast_in_dim.41), calls=%async_computation | async-start | bytes 6291456 | tf_op jit(solution)/shard_map/all_to_all | solution.py:76
  21.7 36.6 %all-to-all-done = bf16[4,96,4096]{2,1,0:T(8,128)(2,1)} async-done(((bf16[4,96,4096]{2,1,0:T(8,128)(2,1)}), bf16[4,96,4096]{2,1,0:T(8,128)(2,1)}, u32[]{:S(2)}, u32[]{:S(2)}) %all-to-all-start) | async-done | bytes 3145760 | tf_op jit(solution)/shard_map/all_to_all | solution.py:76
  58.2 2.9 %fusion.202 = f32[384,2,4]{0,2,1:T(4,128)S(1)} fusion(bf16[384,4096,1]{1,0,2:T(8,128)(2,1)} %bitcast.23, bf16[2,4,4096]{2,1,0:T(4,128)(2,1)S(1)} %dot_general.67), kind=kOutput, calls=%fused_computation.337 | convolution fusion | flops 25165824 | bytes 3223552 | tf_op jit(solution)/shard_map/dot_general | solution.py:275
  61.9 3.1 %convolution_convert_fusion = bf16[384,128]{1,0:T(8,128)(2,1)S(1)} fusion(bf16[384,4096]{1,0:T(8,128)(2,1)} %bitcast.14, bf16[4096,768]{1,0:T(8,128)(2,1)} %all-gather.10.cloned.1.call-done), kind=kOutput, calls=%fused_computation.105 | convolution fusion | flops 402702336 | bytes 4292608 | tf_op jit(solution)/shard_map/dot_general | solution.py:282
  65.1 2.1 collective-permute-start.1
  67.2 4.9 %fusion.57 = bf16[384,512]{1,0:T(8,128)(2,1)S(1)} fusion(bf16[384,4096]{1,0:T(8,128)(2,1)} %bitcast.14, bf16[4096,768]{1,0:T(8,128)(2,1)} %all-gather.10.cloned.1.call-done), kind=kOutput, calls=%fused_computation.88 | convolution fusion | flops 1610809344 | bytes 7733248 | tf_op jit(solution)/shard_map/dot_general | solution.py:282
  72.2 3.3 %convolution_convert_fusion.1 = bf16[384,128]{1,0:T(8,128)(2,1)S(1)} fusion(bf16[384,4096]{1,0:T(8,128)(2,1)} %bitcast.14, bf16[4096,768]{1,0:T(8,128)(2,1)} %all-gather.10.cloned.1.call-done), kind=kOutput, calls=%fused_computation.106 | convolution fusion | flops 402702336 | bytes 4292608 | tf_op jit(solution)/shard_map/dot_general | solution.py:282
  76.3 3.0 %collective-permute-start = (bf16[128,128]{1,0:T(8,128)(2,1)S(1)}, bf16[128,128]{1,0:T(8,128)(2,1)S(1)}, u32[]{:S(2)}, u32[]{:S(2)}) collective-permute-start(bf16[128,128]{1,0:T(8,128)(2,1)S(1)} %slice.295), channel_id=1, source_target_pairs={{0,4},{4,8},{8,12},{12,16},{16,20},{20,24},{24,28},{28,32},{32,36}... | collective-permute-start | bytes 98312 | tf_op jit(solution)/shard_map/ppermute | solution.py:24
  79.7 0.7 fusion.36
  80.6 1.6 copy-done.1
  83.7 2.8 %fusion.60 = bf16[3,128,2,4,64]{1,4,3,2,0:T(8,128)(2,1)S(1)} fusion(f32[3,2,256,128,4]{3,2,4,1,0:T(8,128)} %copy-done.1, f32[3,2,4,128]{3,2,1,0:T(4,128)S(1)} %exponential_add_fusion, f32[3,2,4,128]{3,2,1,0:T(4,128)S(1)} %broadcast_maximum_fusion, pred[3,128,256]{1,2,0:T(8,128)(4,1)S(1)} %fusion.110, bf16[3,128,2,64]{1,3,2,0:T(8,128)(2,1)S(1)} %copy.101, ...), kind=kOutput, calls=%fused_computation.89 | convolution fusion | flops 105185280 | bytes 3858432 | tf_op jit(solution)/shard_map/nhgqk,nkhd->nqhgd/dot_general | solution.py:196
  87.0 1.3 broadcast_in_dim.44
  88.3 3.7 %all-to-all-start.1 = ((bf16[4,384,512]{1,2,0:T(8,128)(2,1)}), bf16[4,384,512]{1,2,0:T(8,128)(2,1)S(1)}, u32[]{:S(2)}, u32[]{:S(2)}) async-start(bf16[4,384,512]{1,2,0:T(8,128)(2,1)} %broadcast_in_dim.44), calls=%async_computation.1 | async-start | bytes 3145728 | tf_op jit(solution)/shard_map/all_to_all | solution.py:76
  92.0 23.7 %all-gather.12.cloned.1.call-done = bf16[4096,1024]{1,0:T(8,128)(2,1)} async-done(((bf16[128,1024]{1,0:T(8,128)(2,1)}), bf16[4096,1024]{1,0:T(8,128)(2,1)}) %all-gather.12.cloned.1.call-update) | async-done | bytes 8388624 | tf_op jit(solution)/shard_map/all_gather | solution.py:96
  115.7 3.5 %fusion.64 = f32[384,256]{1,0:T(8,128)S(1)} fusion(bf16[384,4096]{1,0:T(8,128)(2,1)} %bitcast.14, bf16[4096,1024]{1,0:T(8,128)(2,1)} %all-gather.12.cloned.1.call-done), kind=kOutput, calls=%fused_computation.91 | convolution fusion | flops 805502976 | bytes 5636096 | tf_op jit(solution)/shard_map/dot_general | solution.py:282
  119.6 3.5 %fusion.73 = f32[384,256]{1,0:T(8,128)S(1)} fusion(bf16[384,4096]{1,0:T(8,128)(2,1)} %bitcast.14, bf16[4096,1024]{1,0:T(8,128)(2,1)} %all-gather.12.cloned.1.call-done), kind=kOutput, calls=%fused_computation.94 | convolution fusion | flops 805601280 | bytes 5636096 | tf_op jit(solution)/shard_map/dot_general | solution.py:282
  123.5 4.6 %while.32 = (s32[]{:T(128)}, f32[4,64,64]{2,1,0:T(8,128)S(1)}, f32[4,64]{1,0:T(4,128)S(1)}, f32[4]{0:T(128)S(1)}, f32[3,4,128]{2,1,0:T(4,128)S(1)}, /*index=5*/f...) while((s32[]{:T(128)}, f32[4,64,64]{2,1,0:T(8,128)S(1)}, ...), condition=%wide.region_6.7_spmd.clone, body=%wide.region_3.6_spmd.clone.sunk | while | flops 25709840 | bytes 618317 | solution.py:238
  128.6 1.9 all-gather.3
  131.8 12.6 %all-gather.4 = bf16[4,262,64]{1,2,0:T(8,128)(2,1)S(1)} all-gather(bf16[1,262,64]{1,2,0:T(8,128)(2,1)S(1)} %maximum_bitcast_fusion.5), channel_id=3, replica_groups=mesh['sp_0'=4,'sp_1'=4,'sp_2'=2,'tp'=4] {'sp_1'}, dimensions={0}, use_global_device_ids=true | all-gather | bytes 167680 | tf_op jit(solution)/shard_map/all_gather | solution.py:41
  146.4 12.8 %all-gather.5 = bf16[4,262,64]{1,2,0:T(8,128)(2,1)S(1)} all-gather(bf16[1,262,64]{1,2,0:T(8,128)(2,1)S(1)} %maximum_bitcast_fusion.6), channel_id=4, replica_groups=mesh['sp_0'=4,'sp_1'=4,'sp_2'=2,'tp'=4] {'sp_0'}, dimensions={0}, use_global_device_ids=true | all-gather | bytes 167680 | tf_op jit(solution)/shard_map/all_gather | solution.py:41
  160.4 0.8 copy.173
  161.1 0.8 copy.174
  161.9 0.7 copy.175
  162.6 0.7 copy.176
  163.4 0.7 copy.177
  164.1 0.7 copy.178
  164.9 0.8 copy.179
  165.6 0.7 copy.180
  166.4 0.8 copy.181
  167.1 0.8 copy.182
  167.9 3.5 %fusion.79 = f32[384,256]{1,0:T(8,128)S(1)} fusion(bf16[384,4096]{1,0:T(8,128)(2,1)} %bitcast.14, bf16[4096,1024]{1,0:T(8,128)(2,1)} %all-gather.12.cloned.1.call-done), kind=kOutput, calls=%fused_computation.96 | convolution fusion | flops 805502976 | bytes 5636096 | tf_op jit(solution)/shard_map/dot_general | solution.py:282
  171.8 1.8 multiply_add_fusion.1
  173.6 14.6 %while.31 = (s32[]{:T(128)}, f32[4,64,64]{2,1,0:T(8,128)S(1)}, f32[4,64]{1,0:T(4,128)S(1)}, f32[4]{0:T(128)S(1)}, f32[3,4,128,64]{2,3,1,0:T(8,128)}, /*index=5*/...) while((s32[]{:T(128)}, f32[4,64,64]{2,1,0:T(8,128)S(1)}, ...), condition=%wide.region_13.14_spmd, body=%wide.region_8.13_spmd.sunk | while | flops 152689152 | bytes 2611085 | solution.py:242
  176.7 1.0 fusion.258
  178.5 0.7 dynamic-slice_bitcast_fusion.6
  181.6 1.0 fusion.258
  186.4 1.0 fusion.258
  188.2 1.3 copy.183
  190.0 3.6 %fusion.103 = bf16[384,256]{1,0:T(8,128)(2,1)S(1)} fusion(f32[384,256]{1,0:T(8,128)S(1)} %reshape.1781, bf16[384,4096]{1,0:T(8,128)(2,1)} %bitcast.14, bf16[4096,1024]{1,0:T(8,128)(2,1)} %all-gather.12.cloned.1.call-done), kind=kOutput, calls=%fused_computation.104 | convolution fusion | flops 805994496 | bytes 5832704 | tf_op jit(solution)/shard_map/dot_general | solution.py:282
  193.7 0.9 broadcast_in_dim.49
  194.7 4.4 %all-to-all-start.2 = ((bf16[4,384,256]{1,2,0:T(8,128)(2,1)}), bf16[4,384,256]{1,2,0:T(8,128)(2,1)S(1)}, u32[]{:S(2)}, u32[]{:S(2)}) async-start(bf16[4,384,256]{1,2,0:T(8,128)(2,1)} %broadcast_in_dim.49), calls=%async_computation.2 | async-start | bytes 1572864 | tf_op jit(solution)/shard_map/all_to_all | solution.py:76
  199.8 8.8 %all-to-all-done.2 = bf16[4,384,256]{1,2,0:T(8,128)(2,1)S(1)} async-done(((bf16[4,384,256]{1,2,0:T(8,128)(2,1)}), bf16[4,384,256]{1,2,0:T(8,128)(2,1)S(1)}, u32[]{:S(2)}, u32[]{:S(2)}) %all-to-all-start.2) | async-done | bytes 786464 | tf_op jit(solution)/shard_map/all_to_all | solution.py:76
  208.6 6.3 %fusion.53 = bf16[384,1024]{1,0:T(8,128)(2,1)} fusion(bf16[3072,1024]{1,0:T(8,128)(2,1)} %all-gather.14.cloned.1.call-done, bf16[384,1024]{0,1:T(8,128)(2,1)S(1)} %bitcast.535, bf16[384,2048]{0,1:T(8,128)(2,1)S(1)} %bitcast.533), kind=kOutput, calls=%fused_computation.86 | convolution fusion | flops 2421030912 | bytes 9437184 | tf_op jit(solution)/shard_map/dot_general | solution.py:297
  (270 shorter events, 27.3 us)
Async XLA Ops:
  7.2 14.2 %copy-start = (bf16[4096,2,16]{0,2,1:T(8,128)(2,1)S(1)}, bf16[4096,2,16]{0,2,1:T(8,128)(2,1)}, u32[]{:S(2)}) copy-start(bf16[4096,2,16]{0,2,1:T(8,128)(2,1)} %param.27) | copy-start | bytes 786436
  7.2 54.7 %all-gather.10.cloned.1.call-start = ((), (), s32[]{:S(2)}) async-start(), calls=%async_computation.3 | async-start | bytes 6488064 | tf_op jit(solution)/shard_map/all_gather | solution.py:96
  8.9 106.8 %all-gather.12.cloned.1.call-start = ((), (), s32[]{:S(2)}) async-start(), calls=%async_computation.4 | async-start | bytes 8650752 | tf_op jit(solution)/shard_map/all_gather | solution.py:96
  15.6 5.6 %copy-start.37 = (f32[8]{0:T(128)S(1)}, f32[8]{0:T(128)}, u32[]{:S(2)}) copy-start(f32[8]{0:T(128)} %param.28) | copy-start | bytes 100
  15.6 42.6 %all-to-all-start = ((bf16[4,96,4096]{2,1,0:T(8,128)(2,1)}), bf16[4,96,4096]{2,1,0:T(8,128)(2,1)}, u32[]{:S(2)}, u32[]{:S(2)}) async-start(bf16[4,96,4096]{2,1,0:T(8,128)(2,1)} %broadcast_in_dim.41), calls=%async_computation | async-start | bytes 6291456 | tf_op jit(solution)/shard_map/all_to_all | solution.py:76
  20.4 40.7 %copy-start.21 = (f32[384,4]{0,1:T(4,128)S(1)}, f32[384,4]{0,1:T(4,128)}, u32[]{:S(2)}) copy-start(f32[384,4]{0,1:T(4,128)} %param.30) | copy-start | bytes 18436
  20.4 40.7 %copy-start.36 = (f32[4]{0:T(128)S(1)}, f32[4]{0:T(128)}, u32[]{:S(2)}) copy-start(f32[4]{0:T(128)} %param.29) | copy-start | bytes 52
  20.4 179.4 %all-gather.14.cloned.1.call-start = ((), (), s32[]{:S(2)}) async-start(), calls=%async_computation.5 | async-start | bytes 6488064 | tf_op jit(solution)/shard_map/all_gather | solution.py:268
  21.3 61.5 %copy-start.7 = (f32[2,4]{1,0:T(2,128)}, f32[2,4]{1,0:T(2,128)S(1)}, u32[]{:S(2)}) copy-start(f32[2,4]{1,0:T(2,128)S(1)} %max.684) | copy-start | bytes 100
  65.1 14.4 %collective-permute-start.1 = (bf16[128,128]{1,0:T(8,128)(2,1)S(1)}, bf16[128,128]{1,0:T(8,128)(2,1)S(1)}, u32[]{:S(2)}, u32[]{:S(2)}) collective-permute-start(bf16[128,128]{1,0:T(8,128)(2,1)S(1)} %slice.296), channel_id=1, source_target_pairs={{0,4},{4,8},{8,12},{12,16},{16,20},{20,24},{24,28},{28,32},{32,36}... | collective-permute-start | bytes 98312 | tf_op jit(solution)/shard_map/ppermute | solution.py:24
  76.3 7.1 %collective-permute-start = (bf16[128,128]{1,0:T(8,128)(2,1)S(1)}, bf16[128,128]{1,0:T(8,128)(2,1)S(1)}, u32[]{:S(2)}, u32[]{:S(2)}) collective-permute-start(bf16[128,128]{1,0:T(8,128)(2,1)S(1)} %slice.295), channel_id=1, source_target_pairs={{0,4},{4,8},{8,12},{12,16},{16,20},{20,24},{24,28},{28,32},{32,36}... | collective-permute-start | bytes 98312 | tf_op jit(solution)/shard_map/ppermute | solution.py:24
  80.5 1.7 copy-start.1
  80.5 2.4 %copy-start.5 = (f32[3,2,4,128]{3,2,1,0:T(4,128)}, f32[3,2,4,128]{3,2,1,0:T(4,128)S(1)}, u32[]{:S(2)}) copy-start(f32[3,2,4,128]{3,2,1,0:T(4,128)S(1)} %get-tuple-element.296) | copy-start | bytes 36868
  82.8 0.6 copy-start.3
  88.3 105.4 %all-to-all-start.1 = ((bf16[4,384,512]{1,2,0:T(8,128)(2,1)}), bf16[4,384,512]{1,2,0:T(8,128)(2,1)S(1)}, u32[]{:S(2)}, u32[]{:S(2)}) async-start(bf16[4,384,512]{1,2,0:T(8,128)(2,1)} %broadcast_in_dim.44), calls=%async_computation.1 | async-start | bytes 3145728 | tf_op jit(solution)/shard_map/all_to_all | solution.py:76
  128.2 31.6 %copy-start.2 = (f32[3,4,128]{2,1,0:T(4,128)}, f32[3,4,128]{2,1,0:T(4,128)S(1)}, u32[]{:S(2)}) copy-start(f32[3,4,128]{2,1,0:T(4,128)S(1)} %get-tuple-element.517) | copy-start | bytes 18436
  130.7 29.1 %copy-start.9 = (f32[4]{0:T(128)}, f32[4]{0:T(128)S(1)}, u32[]{:S(2)}) copy-start(f32[4]{0:T(128)S(1)} %get-tuple-element.248) | copy-start | bytes 52
  130.7 29.1 %copy-start.10 = (f32[4]{0:T(128)}, f32[4]{0:T(128)S(1)}, u32[]{:S(2)}) copy-start(f32[4]{0:T(128)S(1)} %get-tuple-element.291) | copy-start | bytes 52
  130.8 29.1 %copy-start.11 = (f32[4]{0:T(128)}, f32[4]{0:T(128)S(1)}, u32[]{:S(2)}) copy-start(f32[4]{0:T(128)S(1)} %get-tuple-element.293) | copy-start | bytes 52
  130.8 29.1 %copy-start.12 = (f32[4]{0:T(128)}, f32[4]{0:T(128)S(1)}, u32[]{:S(2)}) copy-start(f32[4]{0:T(128)S(1)} %get-tuple-element.294) | copy-start | bytes 52
  144.7 15.2 %copy-start.13 = (f32[4]{0:T(128)}, f32[4]{0:T(128)S(1)}, u32[]{:S(2)}) copy-start(f32[4]{0:T(128)S(1)} %get-tuple-element.243) | copy-start | bytes 52
  144.7 15.2 %copy-start.14 = (f32[4]{0:T(128)}, f32[4]{0:T(128)S(1)}, u32[]{:S(2)}) copy-start(f32[4]{0:T(128)S(1)} %get-tuple-element.280) | copy-start | bytes 52
  144.7 15.2 %copy-start.15 = (f32[4]{0:T(128)}, f32[4]{0:T(128)S(1)}, u32[]{:S(2)}) copy-start(f32[4]{0:T(128)S(1)} %get-tuple-element.281) | copy-start | bytes 52
  144.7 15.2 %copy-start.16 = (f32[4]{0:T(128)}, f32[4]{0:T(128)S(1)}, u32[]{:S(2)}) copy-start(f32[4]{0:T(128)S(1)} %get-tuple-element.282) | copy-start | bytes 52
  144.7 15.2 %copy-start.17 = (f32[4]{0:T(128)}, f32[4]{0:T(128)S(1)}, u32[]{:S(2)}) copy-start(f32[4]{0:T(128)S(1)} %get-tuple-element.284) | copy-start | bytes 52
  144.7 15.2 %copy-start.18 = (f32[4]{0:T(128)}, f32[4]{0:T(128)S(1)}, u32[]{:S(2)}) copy-start(f32[4]{0:T(128)S(1)} %get-tuple-element.285) | copy-start | bytes 52
  144.7 15.2 %copy-start.19 = (f32[4]{0:T(128)}, f32[4]{0:T(128)S(1)}, u32[]{:S(2)}) copy-start(f32[4]{0:T(128)S(1)} %get-tuple-element.286) | copy-start | bytes 52
  144.8 15.2 %copy-start.20 = (f32[4]{0:T(128)}, f32[4]{0:T(128)S(1)}, u32[]{:S(2)}) copy-start(f32[4]{0:T(128)S(1)} %get-tuple-element.287) | copy-start | bytes 52
  159.5 0.5 copy-start.22
  159.5 0.6 copy-start.23
  159.5 0.6 copy-start.31
  159.5 0.6 copy-start.32
  159.6 0.6 copy-start.33
  159.6 0.6 copy-start.34
  159.6 0.6 copy-start.35
  159.6 0.6 copy-start.24
  159.6 0.6 copy-start.25
  159.6 0.6 copy-start.26
  159.6 0.6 copy-start.27
  159.7 0.6 copy-start.28
  159.7 0.6 copy-start.29
  159.7 0.6 copy-start.30
  190.0 9.1 %copy-start.4 = (f32[3,2,4,128]{3,2,1,0:T(4,128)S(1)}, f32[3,2,4,128]{3,2,1,0:T(4,128)}, u32[]{:S(2)}) copy-start(f32[3,2,4,128]{3,2,1,0:T(4,128)} %copy-done.3) | copy-start | bytes 36868
  190.0 9.1 %copy-start.6 = (f32[3,2,4,128]{3,2,1,0:T(4,128)S(1)}, f32[3,2,4,128]{3,2,1,0:T(4,128)}, u32[]{:S(2)}) copy-start(f32[3,2,4,128]{3,2,1,0:T(4,128)} %copy-done.5) | copy-start | bytes 36868
  190.0 9.1 %copy-start.8 = (f32[2,4]{1,0:T(2,128)S(1)}, f32[2,4]{1,0:T(2,128)}, u32[]{:S(2)}) copy-start(f32[2,4]{1,0:T(2,128)} %copy-done.7) | copy-start | bytes 100
  194.7 13.9 %all-to-all-start.2 = ((bf16[4,384,256]{1,2,0:T(8,128)(2,1)}), bf16[4,384,256]{1,2,0:T(8,128)(2,1)S(1)}, u32[]{:S(2)}, u32[]{:S(2)}) async-start(bf16[4,384,256]{1,2,0:T(8,128)(2,1)} %broadcast_in_dim.49), calls=%async_computation.2 | async-start | bytes 1572864 | tf_op jit(solution)/shard_map/all_to_all | solution.py:76
Sparse Core Ops, SparseCore 0:
  10.2 51.6 all-gather.9
  64.2 51.5 all-gather.11
  118.0 49.9 all-gather.13
where the time goes:
time: 222 us; the launch traced here: 221 us
  waiting for transfers between devices  70.2 us (32%)
  matrix products  48.7 us (22%)
  blocking collectives  27.3 us (12%)
  local copies, waits for them, and re-layouts  26.5 us (12%)
  starting transfers between devices  18.2 us (8%)
  other arithmetic  15.5 us (7%)
  between operations  14.7 us (7%)
    all_to_all x3, waiting for transfers between devices, from_everyone(): return lax.all_to_all(copies, axis, split_axis=0, concat_axis=0, tiled=True)  45.3 us
    all_gather x3, blocking collectives, collected_together(): both, at, found = (lax.all_gather(jnp.concatenate(lines), axis), 0, {})  27.3 us
    dot_general x7, matrix products, add_pieces(): jnp.dot(token_rows, segment, preferred_element_type=jnp.float32)  25.5 us
    all_gather x2, waiting for transfers between devices, in_one_piece(): lax.all_gather(both, axis, axis=dim, tiled=True)  24.2 us
    all_to_all x3, starting transfers between devices, from_everyone(): return lax.all_to_all(copies, axis, split_axis=0, concat_axis=0, tiled=True)  13 us
    convert_element_type x10, local copies, waits for them, and re-layouts, entering(): part[k].astype(own.dtype)  7.52 us
    dot_general x1, matrix products, shards(): mixed = jnp.dot(joined, out_whole, preferred_element_type=jnp.float32)  6.28 us
    ppermute x2, starting transfers between devices, passed_along(): return lax.ppermute(block, axis, route)  5.14 us
  transfers between devices with their start and end apart: 8, of which 4 were waited for; matrix products, arithmetic and copies ran while one was open for 36% of the time, Pallas kernels for 0%

commit v1 on v0

--- a/solution.py
+++ b/solution.py
@@ -1,21 +1,299 @@
+import functools
 import math
 
 import jax
 import jax.numpy as jnp
 from jax import lax
+from jax.experimental import pallas as pl
+from jax.experimental.pallas import tpu as pltpu
 from jax.sharding import Mesh
 from jax.sharding import PartitionSpec as P
 
 HD = 64
 WINDOW = 128
 BLK = 128
-SP = ("sp_0", "sp_1", "sp_2")
-SP_TP = ("sp_0", "sp_1", "sp_2", "tp")
-
-
 EPSILON = 1e-06
 MASKED = -1e30
 exact_precision = lax.Precision.HIGHEST
+MESH = pl.DeviceIdType.MESH
+RING = 4
+TOK = 96
+ROWS = 8 * TOK
+D = 4096
+PLANE = ("z", "y")
+MAX_COPIES = 192
+
+
+class Wires:
+    def __init__(self, send_sem, recv_sem):
+        self.send_sem, self.recv_sem = send_sem, recv_sem
+        self.count = 0
+        self.started = []
+        z, y, c, x = (lax.axis_index(a) for a in ("z", "y", "c", "x"))
+        self.at = {"z": z, "y": y, "c": c, "x": x}
+
+    def moved(self, **new):
+        where = dict(self.at)
+        where.update(new)
+        return (where["z"], where["y"], where["c"], where["x"])
+
+    def step(self, axis, distance):
+        return lax.rem(self.at[axis] + distance + RING, RING)
+
+    def neighbour(self, axis, distance):
+        return self.moved(**{axis: self.step(axis, distance)})
+
+    def partner(self):
+        return self.moved(c=1 - self.at["c"])
+
+    def send(self, src, dst, device):
+        k = self.count
+        self.count += 1
+        copy = pltpu.make_async_remote_copy(
+            src_ref=src,
+            dst_ref=dst,
+            send_sem=self.send_sem.at[k],
+            recv_sem=self.recv_sem.at[k],
+            device_id=device,
+            device_id_type=MESH,
+        )
+        copy.start()
+        self.started.append(copy)
+        return k
+
+    def arrived(self, k, dst):
+        pltpu.make_async_remote_copy(
+            src_ref=dst,
+            dst_ref=dst,
+            send_sem=self.send_sem.at[k],
+            recv_sem=self.recv_sem.at[k],
+            device_id=self.partner(),
+            device_id_type=MESH,
+        ).wait_recv()
+
+    def finish(self):
+        for copy in self.started:
+            copy.wait_send()
+
+
+class PlaneGather:
+    def __init__(self, wires, whole, depth, core):
+        self.w, self.whole, self.depth, self.core = wires, whole, depth, core
+        self.first, self.second = ("z", "y") if core == 0 else ("y", "z")
+        self.sent = {}
+
+    def rows(self, d1, d2, part=None):
+        i1, i2 = self.w.step(self.first, d1), self.w.step(self.second, d2)
+        z, y = (i1, i2) if self.core == 0 else (i2, i1)
+        start = ((z * RING + y) * 2 + self.core) * self.depth
+        half = self.depth // 2
+        if part is None:
+            return self.whole.at[pl.ds(pl.multiple_of(start, 16), self.depth)]
+        return self.whole.at[pl.ds(pl.multiple_of(start + part * half, 16), half)]
+
+    def go(self, name, d1, d2, axis, distance, part=None):
+        block = self.rows(d1, d2, part)
+        self.sent[name] = self.w.send(block, block, self.w.neighbour(axis, distance))
+
+    def came(self, name, d1, d2, part=None):
+        self.w.arrived(self.sent[name], self.rows(d1, d2, part))
+
+    def second_round(self, d1):
+        self.go(("b+", d1), d1, 0, self.second, 1)
+        self.go(("b-", d1), d1, 0, self.second, -1)
+
+    def start_first(self):
+        self.go("a+", 0, 0, self.first, 1)
+        self.go("a-", 0, 0, self.first, -1)
+
+    def start_second(self):
+        self.second_round(0)
+
+    def first_came(self):
+        self.came("a+", -1, 0)
+        self.go("ah+", -1, 0, self.first, 1, 0)
+        self.second_round(-1)
+        self.came("a-", 1, 0)
+        self.go("ah-", 1, 0, self.first, -1, 1)
+        self.second_round(1)
+
+    def second_came(self, d1):
+        self.came(("b+", d1), d1, -1)
+        self.go(("bh+", d1), d1, -1, self.second, 1, 0)
+        self.came(("b-", d1), d1, 1)
+        self.go(("bh-", d1), d1, 1, self.second, -1, 1)
+
+    def first_done(self):
+        self.came("ah+", 2, 0, 0)
+        self.came("ah-", 2, 0, 1)
+        self.second_round(2)
+
+    def second_done(self, d1):
+        self.came(("bh+", d1), d1, 2, 0)
+        self.came(("bh-", d1), d1, 2, 1)
+
+
+def plane_steps(wires, whole, depth):
+    pair = [PlaneGather(wires, whole, depth, core) for core in (0, 1)]
+    steps = []
+    for name in ("start_first", "start_second", "first_came"):
+        steps += [functools.partial(getattr(g, name)) for g in pair]
+    steps += [functools.partial(g.second_came, 0) for g in pair]
+    steps += [g.first_done for g in pair]
+    for d1 in (-1, 1, 2):
+        steps += [functools.partial(g.second_came, d1) for g in pair]
+    for d1 in (0, -1, 1, 2):
+        steps += [functools.partial(g.second_done, d1) for g in pair]
+    return steps
+
+
+class TokenGather:
+    def __init__(self, wires, whole):
+        self.w, self.whole = wires, whole
+
+    def rows(self, dx, other=False, part=None):
+        c = self.w.at["c"]
+        c = 1 - c if other else c
+        start = (c * RING + self.w.step("x", dx)) * TOK
+        half = TOK // 2
+        if part is None:
+            return self.whole.at[pl.ds(pl.multiple_of(start, 16), TOK)]
+        return self.whole.at[pl.ds(pl.multiple_of(start + part * half, 16), half)]
+
+    def start(self):
+        own = self.rows(0)
+        self.right = self.w.send(own, own, self.w.neighbour("x", 1))
+        self.left = self.w.send(own, own, self.w.neighbour("x", -1))
+        self.over = {0: self.w.send(own, own, self.w.partner())}
+
+    def came(self):
+        w = self.w
+        for k, dx, part in ((self.right, -1, 0), (self.left, 1, 1)):
+            block = self.rows(dx)
+            w.arrived(k, block)
+            piece = self.rows(dx, part=part)
+            k2 = w.send(piece, piece, w.neighbour("x", -dx))
+            if dx < 0:
+                self.right2 = k2
+            else:
+                self.left2 = k2
+            self.over[dx] = w.send(block, block, w.partner())
+
+    def done(self):
+        w = self.w
+        w.arrived(self.right2, self.rows(2, part=0))
+        w.arrived(self.left2, self.rows(2, part=1))
+        block = self.rows(2)
+        self.over[2] = w.send(block, block, w.partner())
+        for dx in (0, -1, 1, 2):
+            w.arrived(self.over[dx], self.rows(dx, other=True))
+
+
+def gather_kernel(
+    tok, gain, wq, wk, wv, wmq, wmk, wmv, wmg, wo,
+    normed, w1, w2, w3,
+    kv, send_sem, recv_sem, local_sem,
+):
+    w = Wires(send_sem, recv_sem)
+    z, y, c = w.at["z"], w.at["y"], w.at["c"]
+    barrier = pltpu.get_barrier_semaphore()
+    greeted = [w.neighbour(a, d) for a in ("z", "y", "x") for d in (1, -1)] + [w.partner()]
+    for device in greeted:
+        pl.semaphore_signal(barrier, inc=1, device_id=device, device_id_type=MESH)
+
+    kv[0] = jnp.concatenate([wk[:, :HD], wv[:, :HD]], axis=1)
+    kv[1] = jnp.concatenate([wk[:, HD:], wv[:, HD:]], axis=1)
+    values = tok[...].astype(jnp.float32)
+    rescale = lax.rsqrt(jnp.mean(values * values, axis=-1, keepdims=True) + EPSILON)
+    own_rows = pl.ds(pl.multiple_of((c * RING + w.at["x"]) * TOK, 16), TOK)
+    normed[own_rows, :] = (values * rescale * gain[...]).astype(jnp.bfloat16)
+    pl.semaphore_wait(barrier, len(greeted))
+
+    block = (z * RING + y) * 2 + c
+    r128 = pl.ds(pl.multiple_of(block * 128, 128), 128)
+    r96 = pl.ds(pl.multiple_of(block * 96, 16), 96)
+
+    def cut(ref, width):
+        return lambda h: ref.at[:, pl.ds(pl.multiple_of(h * width, 128), width)]
+
+    pieces = [
+        (cut(wmk, 128), w1.at[r128, 0:128]),
+        (cut(wmv, 128), w1.at[r128, 128:256]),
+        (lambda h: kv.at[h], w1.at[r128, 256:384]),
+        (cut(wq, 256), w2.at[r128, 0:256]),
+        (cut(wmq, 128), w2.at[r128, 256:384]),
+        (cut(wmg, 128), w2.at[r128, 384:512]),
+        (cut(wo, 512), w3.at[r96, :]),
+    ]
+    local = []
+    over = []
+    for n, (half_of, dst) in enumerate(pieces):
+        copy = pltpu.make_async_copy(half_of(c), dst, local_sem.at[n])
+        copy.start()
+        local.append(copy)
+        over.append(w.send(half_of(1 - c), dst, w.partner()))
+
+    theirs = (z * RING + y) * 2 + 1 - c
+    t128 = pl.ds(pl.multiple_of(theirs * 128, 128), 128)
+    t96 = pl.ds(pl.multiple_of(theirs * 96, 16), 96)
+    landing = [
+        w1.at[t128, 0:128], w1.at[t128, 128:256], w1.at[t128, 256:384],
+        w2.at[t128, 0:256], w2.at[t128, 256:384], w2.at[t128, 384:512], w3.at[t96, :],
+    ]
+    tokens = TokenGather(w, normed)
+    tokens.start()
+    for n, copy in enumerate(local):
+        copy.wait()
+        w.arrived(over[n], landing[n])
+
+    g1 = plane_steps(w, w1, 128)
+    g2 = plane_steps(w, w2, 128)
+    g3 = plane_steps(w, w3, 96)
+    for step in g1[:8]:
+        step()
+    for step in g2[:4]:
+        step()
+    for step in g1[8:12]:
+        step()
+    tokens.came()
+    for step in g1[12:]:
+        step()
+    for step in g3[:4]:
+        step()
+    for step in g2[4:12]:
+        step()
+    tokens.done()
+    for step in g2[12:]:
+        step()
+    for step in g3[4:]:
+        step()
+    w.finish()
+
+
+def gather_all(tok, gain, wq, wk, wv, wmq, wmk, wmv, wmg, wo):
+    vmem = pl.BlockSpec(memory_space=pltpu.VMEM)
+    bf = jnp.bfloat16
+    return pl.pallas_call(
+        gather_kernel,
+        out_shape=[
+            jax.ShapeDtypeStruct((ROWS, D), bf),
+            jax.ShapeDtypeStruct((D, 384), bf),
+            jax.ShapeDtypeStruct((D, 512), bf),
+            jax.ShapeDtypeStruct((3072, 512), bf),
+        ],
+        in_specs=[vmem] * 10,
+        out_specs=[vmem] * 4,
+        scratch_shapes=[
+            pltpu.VMEM((2, 128, 128), bf),
+            pltpu.SemaphoreType.DMA((MAX_COPIES,)),
+            pltpu.SemaphoreType.DMA((MAX_COPIES,)),
+            pltpu.SemaphoreType.DMA((8,)),
+        ],
+        compiler_params=pltpu.CompilerParams(
+            collective_id=0, has_side_effects=True, vmem_limit_bytes=60 * 1024 * 1024
+        ),
+        name="gather_all",
+    )(tok, gain.reshape(1, D), wq, wk, wv, wmq, wmk, wmv, wmg, wo)
 
 
 def passed_along(block, axis, distance):
@@ -82,26 +360,6 @@
     return pieces.reshape(*shape[:dim], shape[dim] * shape[dim + 1], *shape[dim + 2 :])
 
 
-def gather_directly(x, axis, dim):
-    pieces = from_everyone(x, axis)
-    return joined_along(pieces, dim)
-
-
-def in_one_piece(arrays, axis, dim, along):
-    ends, at = ([], 0)
-    for a in arrays[:-1]:
-        at += a.shape[along]
-        ends.append(at)
-    both = jnp.concatenate(arrays, axis=along)
-    return tuple(jnp.split(lax.all_gather(both, axis, axis=dim, tiled=True), ends, axis=along))
-
-
-def normalize(tokens, norm_gain):
-    values = tokens.astype(jnp.float32)
-    rescale = lax.rsqrt(jnp.mean(values * values, axis=-1, keepdims=True) + EPSILON)
-    return (values * rescale * norm_gain).astype(jnp.bfloat16)
-
-
 def advance(carried, key_block, value_block, in_block, cumulative):
     memory_state, normalizer, stabilizer = carried
     block_total = cumulative[:, -1]
@@ -161,7 +419,7 @@
     group_size = query.shape[1] // HD // kv_local
     block_count = row_count // WINDOW
     rim_key, rim_value = passed_along(
-        (key_rows[row_count - WINDOW :], value_rows[row_count - WINDOW :]), SP, 1
+        (key_rows[row_count - WINDOW :], value_rows[row_count - WINDOW :]), PLANE, 1
     )
     padded_keys = jnp.concatenate([rim_key, key_rows], axis=0).reshape(
         block_count + 1, WINDOW, kv_local, HD
@@ -180,7 +438,7 @@
     distance = query_index - key_index + WINDOW
     in_band = (distance >= 0) & (distance < WINDOW)
     block_index = lax.broadcasted_iota(jnp.int32, (block_count, WINDOW, 2 * WINDOW), 0)
-    key_position = lax.axis_index(SP) * row_count + block_index * WINDOW - WINDOW + key_index[None]
+    key_position = lax.axis_index(PLANE) * row_count + block_index * WINDOW - WINDOW + key_index[None]
     allowed = (in_band[None] & (key_position >= 0))[:, None, None]
     scores = jnp.where(allowed, scores, MASKED)
     sink_logit = sinks.reshape(1, kv_local, group_size, 1, 1)
@@ -203,7 +461,7 @@
     row_count = mem_query.shape[0]
     head_count = forget_bias.shape[0]
     block_count = row_count // BLK
-    sequence_total = row_count * lax.axis_size(SP)
+    sequence_total = row_count * lax.axis_size(PLANE)
 
     def blocks(array):
         return (
@@ -238,7 +496,7 @@
     summary, _ = lax.scan(summarize, initial, (key_blocks, value_blocks, in_blocks, forget_blocks))
     passed = jnp.sum(log_forget, axis=0)
     identity = (jnp.zeros((head_count,), jnp.float32), initial[0], initial[1], initial[2])
-    incoming = entering((passed, summary[0], summary[1], summary[2]), SP, join_states, identity)
+    incoming = entering((passed, summary[0], summary[1], summary[2]), PLANE, join_states, identity)
     _, recall = lax.scan(
         block_step,
         (incoming[1], incoming[2], incoming[3]),
@@ -248,74 +506,51 @@
     return (recall * jax.nn.sigmoid(mem_gate.astype(jnp.float32))).astype(jnp.bfloat16)
 
 
+def swapped(x):
+    return lax.all_to_all(x, "c", split_axis=0, concat_axis=0, tiled=True)
+
+
 def shards(
-    tokens,
-    norm_gain,
-    w_query,
-    w_key,
-    w_value,
-    w_mem_query,
-    w_mem_key,
-    w_mem_value,
-    w_mem_gate,
-    w_gates,
-    sinks,
-    forget_bias,
-    forget_shift,
-    w_out,
+    tokens, norm_gain, w_query, w_key, w_value, w_mem_query, w_mem_key, w_mem_value, w_mem_gate,
+    w_gates, sinks, forget_bias, forget_shift, w_out,
 ):
-    normed = normalize(tokens, norm_gain)
-    out_whole = lax.all_gather(w_out, SP, axis=0, tiled=True)
-    token_rows = gather_directly(normed, "tp", 0)
-    row_count = token_rows.shape[0]
-    head_count = forget_bias.shape[0]
-    gate_columns = lax.dynamic_slice_in_dim(
-        w_gates, lax.axis_index("tp") * head_count, head_count, 2
-    ).reshape(w_gates.shape[0], 2 * head_count)
-    gate_pre = jnp.dot(token_rows, gate_columns, preferred_element_type=jnp.float32).reshape(
-        row_count, 2, head_count
-    )
-
-    def add_pieces(segments):
-        return tuple(
-            (
-                jnp.dot(token_rows, segment, preferred_element_type=jnp.float32)
-                for segment in segments
-            )
-        )
-
-    attn_sums = add_pieces(in_one_piece((w_query, w_key, w_value), SP, 0, 1))
-    attn_parts = [partial_sum.astype(jnp.bfloat16) for partial_sum in attn_sums]
-    attn_out, log_total = attend(attn_parts[0], attn_parts[1], attn_parts[2], sinks)
-    mem_sums = add_pieces(in_one_piece((w_mem_query, w_mem_key, w_mem_value, w_mem_gate), SP, 0, 1))
-    mem_parts = [partial_sum.astype(jnp.bfloat16) for partial_sum in mem_sums]
+    c, x = lax.axis_index("c"), lax.axis_index("x")
+    normed, w1, w2, w3 = gather_all(
+        tokens, norm_gain, w_query, w_key, w_value, w_mem_query, w_mem_key, w_mem_value,
+        w_mem_gate, w_out,
+    )
+    part1 = jnp.dot(normed, w1, preferred_element_type=jnp.float32).astype(jnp.bfloat16)
+    part2 = jnp.dot(normed, w2, preferred_element_type=jnp.float32).astype(jnp.bfloat16)
+    gates = lax.dynamic_slice_in_dim(w_gates, x * 4 + c * 2, 2, 2).reshape(D, 4)
+    gate_pre = jnp.dot(normed, gates, preferred_element_type=jnp.float32).reshape(ROWS, 2, 2)
+    shift = forget_shift.reshape(384, 2, 2).transpose(1, 0, 2).reshape(2 * 384, 2)
+    shift = swapped(shift)
+    attn_out, log_total = attend(
+        part2[:, :256], part1[:, 256:320], part1[:, 320:384], lax.dynamic_slice_in_dim(sinks, c * 4, 4)
+    )
     mem_out = memory(
-        mem_parts[0], mem_parts[1], mem_parts[2], mem_parts[3], gate_pre, forget_bias, forget_shift
-    )
-    head_attn, head_mem = (gather_directly(attn_out, "tp", 1), gather_directly(mem_out, "tp", 1))
-    joined = jnp.concatenate([head_attn, head_mem], axis=1)
-    mixed = jnp.dot(joined, out_whole, preferred_element_type=jnp.float32)
-    return (mixed.astype(jnp.bfloat16), log_total)
+        part2[:, 256:384], part1[:, :128], part1[:, 128:256], part2[:, 384:512],
+        gate_pre, lax.dynamic_slice_in_dim(forget_bias, c * 2, 2), shift,
+    )
+    outs = from_everyone(jnp.concatenate([attn_out, mem_out], axis=1), ("x", "c"))
+    outs = outs.reshape(8, ROWS, 384)
+    joined = jnp.concatenate(
+        [joined_along(outs[:, :, :256], 1), joined_along(outs[:, :, 256:], 1)], axis=1
+    )
+    mixed = jnp.dot(joined, w3, preferred_element_type=jnp.float32).astype(jnp.bfloat16)
+    mixed = swapped(mixed).reshape(2, 384, 512).transpose(1, 0, 2).reshape(384, 1024)
+    log_total = swapped(log_total).reshape(2, 384, 4).transpose(1, 0, 2).reshape(384, 8)
+    return (mixed, log_total)
 
 
 def solution(mesh):
-    torus = Mesh(mesh.devices.reshape(4, 4, 2, mesh.shape["tp"]), ("sp_0", "sp_1", "sp_2", "tp"))
+    torus = Mesh(mesh.devices.reshape(4, 4, 2, mesh.shape["tp"]), ("z", "y", "c", "x"))
+    sp = ("z", "y", "c")
     placed = (
-        P(SP_TP, None),
-        P(),
-        P(SP, "tp"),
-        P(SP, "tp"),
-        P(SP, "tp"),
-        P(SP, "tp"),
-        P(SP, "tp"),
-        P(SP, "tp"),
-        P(SP, "tp"),
-        P(),
-        P("tp"),
-        P("tp"),
-        P(SP, "tp"),
-        P(SP, "tp"),
+        (P(("z", "y", "c", "x"), None), P())
+        + (P(sp, "x"),) * 7
+        + (P(), P("x"), P("x"), P(sp, "x"), P(sp, "x"))
     )
     return jax.shard_map(
-        shards, mesh=torus, in_specs=placed, out_specs=(P(SP, "tp"), P(SP, "tp")), check_vma=False
-    )
+        shards, mesh=torus, in_specs=placed, out_specs=(P(sp, "x"), P(sp, "x")), check_vma=False
+    )

time: 222 us -> 275 us (1.24)
  Pallas kernels: 0 us -> 82.3 us
  waiting for transfers between devices: 70.2 us -> 54 us
  between operations: 14.7 us -> 1.42 us
  matrix products: 48.7 us -> 36.3 us
  other arithmetic: 15.5 us -> 22.5 us
    pallas_call x0 -> x1, Pallas kernels: none -> 82.3 us  [gather_all(): pl.pallas_call(gather_kernel, out_shape=[jax.ShapeDtypeStruct((ROWS, D),...]
    all_gather x3 -> x0, waiting for transfers between devices: 24.2 us -> none  [the longest x2 24.2 us: in_one_piece(): lax.all_gather(both, axis, axis=dim, tiled=True)]
    dot_general x9 -> x4, matrix products: 34.6 us -> 20.9 us  [the longest x1 7.47 us: shards(): jnp.dot(normed, w2, preferred_element_type=jnp.float32).astype(jnp.bfloat16)]
    all_to_all x3 -> x1, waiting for transfers between devices: 45.3 us -> 53.9 us  [from_everyone(): return lax.all_to_all(copies, axis, split_axis=0, concat_axis=0, tiled=True)]
    all_to_all x3 -> x1, starting transfers between devices: 13 us -> 4.59 us  [from_everyone(): return lax.all_to_all(copies, axis, split_axis=0, concat_axis=0, tiled=True)]
    all_to_all x0 -> x2, starting transfers between devices: none -> 7.04 us  [swapped(): return lax.all_to_all(x, 'c', split_axis=0, concat_axis=0, tiled=True)]
    all_to_all x0 -> x1, blocking collectives: none -> 4.37 us  [swapped(): return lax.all_to_all(x, 'c', split_axis=0, concat_axis=0, tiled=True)]
    slice x1 -> x6, local copies, waits for them, and re-layouts: 0.01 us -> 3.83 us  [the longest x1 2.09 us: shards(): outs[:, :, :256]]
  transfers between devices with their start and end apart: 8 -> 5, of which waited for: 4 -> 1; matrix products, arithmetic and copies ran while one was open for 36% -> 23% of each run, Pallas kernels for 0% -> 0%
where the time goes in v1:
time: 275 us; the launch traced here: 273 us
  Pallas kernels  82.3 us (30%)
  waiting for transfers between devices  54 us (20%)
  matrix products  36.3 us (13%)
  blocking collectives  29.4 us (11%)
  local copies, waits for them, and re-layouts  28.9 us (11%)
  other arithmetic  22.5 us (8%)
  starting transfers between devices  17.5 us (6%)
    pallas_call x1, Pallas kernels, gather_all(): pl.pallas_call(gather_kernel, out_shape=[jax.ShapeDtypeStruct((ROWS, D),...  82.3 us
    all_to_all x1, waiting for transfers between devices, from_everyone(): return lax.all_to_all(copies, axis, split_axis=0, concat_axis=0, tiled=True)  53.9 us
    all_gather x2, blocking collectives, collected_together(): both, at, found = (lax.all_gather(jnp.concatenate(lines), axis), 0, {})  25.1 us
    dot_general x1, matrix products, shards(): jnp.dot(normed, w2, preferred_element_type=jnp.float32).astype(jnp.bfloat16)  7.47 us
    all_to_all x2, starting transfers between devices, swapped(): return lax.all_to_all(x, 'c', split_axis=0, concat_axis=0, tiled=True)  7.04 us
    dot_general x1, matrix products, shards(): jnp.dot(normed, w1, preferred_element_type=jnp.float32).astype(jnp.bfloat16)  6.35 us
    ppermute x2, starting transfers between devices, passed_along(): return lax.ppermute(block, axis, route)  5.82 us
  transfers between devices with their start and end apart: 5, of which 1 were waited for; matrix products, arithmetic and copies ran while one was open for 23% of the time, Pallas kernels for 0%

profile of v1, /device:TPU:0, one launch (start us, length us, event | category | flops | bytes accessed | tf_op | source)
XLA Modules:
  0.0 272.7 jit_solution(13217998717927125551)
XLA Ops:
  0.6 82.3 %gather_all.1 = (bf16[768,4096]{1,0:T(8,128)(2,1)}, bf16[4096,384]{1,0:T(8,128)(2,1)}, bf16[4096,512]{1,0:T(8,128)(2,1)}, bf16[3072,512]{1,0:T(8,128)(2,1)}) custom-call(bf16[96,4096]{1,0:T(8,128)(2,1)} %tok.1, f32[1,4096]{1,0:T(1,128)} %bitcast.506, bf16[128,512]{1,0:T(8,128)(2,1)} %wq.1, bf16[128,128]{1,0:T(8,128)(2,1)} %wk.1, bf16[128,128]{1,0:T(8,128)(2,1)} %wv.1, ...), custom_call_target="tpu_custom_call" | custom-call | tf_op jit(solution)/shard_map/gather_all/pallas_call | solution.py:276
  83.0 6.4 %convolution_convert_fusion.1 = bf16[768,384]{0,1:T(8,128)(2,1)S(1)} fusion(bf16[768,4096]{1,0:T(8,128)(2,1)} %get-tuple-element.102, bf16[4096,384]{1,0:T(8,128)(2,1)} %get-tuple-element.103), kind=kOutput, calls=%fused_computation.77 | convolution fusion | flops 2416214016 | bytes 10027008 | tf_op jit(solution)/shard_map/dot_general | solution.py:522
  90.0 2.6 collective-permute-start
  92.6 3.2 %collective-permute-start.1 = (bf16[128,64]{0,1:T(8,128)(2,1)}, bf16[128,64]{0,1:T(8,128)(2,1)}, u32[]{:S(2)}, u32[]{:S(2)}) collective-permute-start(bf16[128,64]{0,1:T(8,128)(2,1)} %get-tuple-element.259), channel_id=1, source_target_pairs={{0,8},{8,16},{16,24},{24,32},{32,40},{40,48},{48,56},{56,64},{64,7... | collective-permute-start | bytes 49160 | tf_op jit(solution)/shard_map/ppermute | solution.py:302
  96.4 3.2 %all-to-all-start = ((f32[2,384,2]{1,2,0:T(2,128)}), f32[2,384,2]{1,2,0:T(2,128)S(1)}, u32[]{:S(2)}, u32[]{:S(2)}) async-start(f32[2,384,2]{1,2,0:T(2,128)} %bitcast.28), calls=%async_computation | async-start | bytes 12288 | tf_op jit(solution)/shard_map/all_to_all | solution.py:510
  99.7 0.6 fusion.63
  100.6 4.5 %fusion.33 = f32[768,2,2]{0,2,1:T(2,128)S(1)} fusion(bf16[2,2,4096]{2,1,0:T(2,128)(2,1)S(1)} %dot_general.51, bf16[768,4096]{1,0:T(8,128)(2,1)} %get-tuple-element.102), kind=kOutput, calls=%fused_computation.61 | convolution fusion | flops 25165824 | bytes 6336512 | tf_op jit(solution)/shard_map/dot_general | solution.py:525
  105.7 8.0 %while.32 = (s32[]{:T(128)}, f32[2,64,64]{2,1,0:T(8,128)S(1)}, f32[2,64]{1,0:T(2,128)S(1)}, f32[2]{0:T(128)S(1)}, f32[6,2,128]{2,1,0:T(2,128)S(1)}, /*index=5*/f...) while((s32[]{:T(128)}, f32[2,64,64]{2,1,0:T(8,128)S(1)}, ...), condition=%wide.region_5.6_spmd.clone, body=%wide.region_2.5_spmd.clone.sunk | while | flops 12854409 | bytes 309985 | solution.py:496
  114.5 12.9 %all-gather.2 = bf16[4,132,64]{1,2,0:T(8,128)(2,1)S(1)} all-gather(bf16[1,132,64]{1,2,0:T(8,128)(2,1)S(1)} %maximum_bitcast_fusion.4), channel_id=2, replica_groups=mesh['z'=4,'y'=4,'c'=2,'x'=4] {'y'}, dimensions={0}, use_global_device_ids=true | all-gather | bytes 84480 | tf_op jit(solution)/shard_map/all_gather | solution.py:319
  129.9 0.7 fusion.114
  131.1 12.2 %all-gather.3 = bf16[4,132,64]{1,2,0:T(8,128)(2,1)S(1)} all-gather(bf16[1,132,64]{1,2,0:T(8,128)(2,1)S(1)} %maximum_bitcast_fusion.5), channel_id=3, replica_groups=mesh['z'=4,'y'=4,'c'=2,'x'=4] {'z'}, dimensions={0}, use_global_device_ids=true | all-gather | bytes 84480 | tf_op jit(solution)/shard_map/all_gather | solution.py:319
  143.3 0.8 slice_reduce_fusion.3
  144.8 7.5 %convolution_convert_fusion = bf16[768,512]{0,1:T(8,128)(2,1)S(1)} fusion(bf16[768,4096]{1,0:T(8,128)(2,1)} %get-tuple-element.102, bf16[4096,512]{1,0:T(8,128)(2,1)} %get-tuple-element.104), kind=kOutput, calls=%fused_computation.75 | convolution fusion | flops 3221618688 | bytes 11272192 | tf_op jit(solution)/shard_map/dot_general | solution.py:523
  152.3 0.7 copy.164
  154.2 0.7 copy.167
  155.1 0.7 copy.153
  155.8 0.7 copy.154
  156.5 0.7 copy.155
  157.2 0.7 copy.156
  157.9 0.7 copy.157
  158.7 0.7 copy.158
  159.5 0.9 fusion.103
  160.3 0.8 subtract_exponential_fusion.10
  161.2 0.9 fusion.83
  162.1 1.2 multiply_add_fusion.1
  163.3 16.8 %while.31 = (s32[]{:T(128)}, f32[2,64,64]{2,1,0:T(8,128)S(1)}, f32[2,64]{1,0:T(2,128)S(1)}, f32[2]{0:T(128)S(1)}, f32[6,2,128,64]{2,3,1,0:T(8,128)S(1)}, /*index...) while((s32[]{:T(128)}, f32[2,64,64]{2,1,0:T(8,128)S(1)}, ...), condition=%wide.region_12.13_spmd, body=%wide.region_7.12_spmd.sunk | while | flops 76352256 | bytes 1332469 | solution.py:500
  180.3 0.8 fusion.54
  181.1 0.9 fusion.53
  182.2 1.2 reshape.1434
  183.6 0.6 copy.98
  184.3 1.4 pad_maximum_fusion.1
  185.9 1.7 fusion.40
  187.7 1.6 fusion.39
  189.3 0.7 fusion.73
  190.0 0.7 exponential_add_fusion
  190.7 3.8 %all-to-all-start.3 = ((f32[2,384,4]{1,2,0:T(4,128)}), f32[2,384,4]{1,2,0:T(4,128)}, u32[]{:S(2)}, u32[]{:S(2)}) async-start(f32[2,384,4]{1,2,0:T(4,128)} %bitcast.100), calls=%async_computation.3 | async-start | bytes 24576 | tf_op jit(solution)/shard_map/all_to_all | solution.py:510
  194.5 1.0 slice.226
  195.6 2.0 fusion.50
  197.9 2.5 broadcast_in_dim.40
  200.4 4.6 %all-to-all-start.1 = ((bf16[8,768,384]{1,2,0:T(8,128)(2,1)}), bf16[8,768,384]{1,2,0:T(8,128)(2,1)}, u32[]{:S(2)}, u32[]{:S(2)}) async-start(bf16[8,768,384]{1,2,0:T(8,128)(2,1)} %broadcast_in_dim.40), calls=%async_computation.1 | async-start | bytes 9437184 | tf_op jit(solution)/shard_map/all_to_all | solution.py:354
  205.0 1.3 reshape.1454
  206.4 53.9 %all-to-all-done.1 = bf16[8,768,384]{1,2,0:T(8,128)(2,1)} async-done(((bf16[8,768,384]{1,2,0:T(8,128)(2,1)}), bf16[8,768,384]{1,2,0:T(8,128)(2,1)}, u32[]{:S(2)}, u32[]{:S(2)}) %all-to-all-start.1) | async-done | bytes 4718624 | tf_op jit(solution)/shard_map/all_to_all | solution.py:354
  260.3 2.1 slice.310
  262.4 1.7 slice.311
  264.1 0.7 copy-done.21
  264.8 2.6 fusion.44
  267.4 4.4 %all_to_all.32 = bf16[2,384,512]{2,1,0:T(8,128)(2,1)S(1)} all-to-all(bf16[2,384,512]{2,1,0:T(8,128)(2,1)S(1)} %bitcast.486), channel_id=1, replica_groups=mesh['z'=4,'y'=4,'c'=2,'x'=4] {'c'}, dimensions={0} | all-to-all | bytes 1572864 | tf_op jit(solution)/shard_map/all_to_all | solution.py:510
  271.8 1.0 copy.168
  (304 shorter events, 33.2 us)
Async XLA Ops:
  0.6 99.8 %copy-start = (bf16[4096,2,16]{0,2,1:T(8,128)(2,1)S(1)}, bf16[4096,2,16]{0,2,1:T(8,128)(2,1)}, u32[]{:S(2)}) copy-start(bf16[4096,2,16]{0,2,1:T(8,128)(2,1)} %param.27) | copy-start | bytes 786436
  83.0 12.8 %copy-start.11 = (f32[384,4]{0,1:T(4,128)S(1)}, f32[384,4]{0,1:T(4,128)}, u32[]{:S(2)}) copy-start(f32[384,4]{0,1:T(4,128)} %param.30) | copy-start | bytes 18436
  90.0 94.4 %collective-permute-start = (bf16[128,64]{0,1:T(8,128)(2,1)}, bf16[128,64]{0,1:T(8,128)(2,1)}, u32[]{:S(2)}, u32[]{:S(2)}) collective-permute-start(bf16[128,64]{0,1:T(8,128)(2,1)} %get-tuple-element.258), channel_id=1, source_target_pairs={{0,8},{8,16},{16,24},{24,32},{32,40},{40,48},{48,56},{56,64},{64,7... | collective-permute-start | bytes 49160 | tf_op jit(solution)/shard_map/ppermute | solution.py:302
  92.6 91.7 %collective-permute-start.1 = (bf16[128,64]{0,1:T(8,128)(2,1)}, bf16[128,64]{0,1:T(8,128)(2,1)}, u32[]{:S(2)}, u32[]{:S(2)}) collective-permute-start(bf16[128,64]{0,1:T(8,128)(2,1)} %get-tuple-element.259), channel_id=1, source_target_pairs={{0,8},{8,16},{16,24},{24,32},{32,40},{40,48},{48,56},{56,64},{64,7... | collective-permute-start | bytes 49160 | tf_op jit(solution)/shard_map/ppermute | solution.py:302
  96.4 8.7 %all-to-all-start = ((f32[2,384,2]{1,2,0:T(2,128)}), f32[2,384,2]{1,2,0:T(2,128)S(1)}, u32[]{:S(2)}, u32[]{:S(2)}) async-start(f32[2,384,2]{1,2,0:T(2,128)} %bitcast.28), calls=%async_computation | async-start | bytes 12288 | tf_op jit(solution)/shard_map/all_to_all | solution.py:510
  100.5 4.6 %copy-start.22 = (f32[4]{0:T(128)S(1)}, f32[4]{0:T(128)}, u32[]{:S(2)}) copy-start(f32[4]{0:T(128)} %param.29) | copy-start | bytes 52
  127.6 3.3 %copy-start.3 = (bf16[4,64]{1,0:T(4,128)(2,1)}, bf16[4,64]{1,0:T(4,128)(2,1)S(1)}, u32[]{:S(2)}) copy-start(bf16[4,64]{1,0:T(4,128)(2,1)S(1)} %get-tuple-element.193) | copy-start | bytes 1540
  127.7 0.6 copy-start.14
  127.7 3.2 %copy-start.4 = (f32[2]{0:T(128)}, f32[2]{0:T(128)S(1)}, u32[]{:S(2)}) copy-start(f32[2]{0:T(128)S(1)} %get-tuple-element.250) | copy-start | bytes 28
  127.7 16.4 %copy-start.10 = (f32[2]{0:T(128)}, f32[2]{0:T(128)S(1)}, u32[]{:S(2)}) copy-start(f32[2]{0:T(128)S(1)} %get-tuple-element.251) | copy-start | bytes 28
  127.7 3.2 %copy-start.5 = (f32[2]{0:T(128)}, f32[2]{0:T(128)S(1)}, u32[]{:S(2)}) copy-start(f32[2]{0:T(128)S(1)} %get-tuple-element.288) | copy-start | bytes 28
  127.8 3.2 %copy-start.6 = (f32[2]{0:T(128)}, f32[2]{0:T(128)S(1)}, u32[]{:S(2)}) copy-start(f32[2]{0:T(128)S(1)} %get-tuple-element.289) | copy-start | bytes 28
  127.8 3.2 %copy-start.7 = (f32[2]{0:T(128)}, f32[2]{0:T(128)S(1)}, u32[]{:S(2)}) copy-start(f32[2]{0:T(128)S(1)} %get-tuple-element.290) | copy-start | bytes 28
  127.8 16.4 %copy-start.12 = (f32[2]{0:T(128)}, f32[2]{0:T(128)S(1)}, u32[]{:S(2)}) copy-start(f32[2]{0:T(128)S(1)} %get-tuple-element.253) | copy-start | bytes 28
  127.8 16.4 %copy-start.15 = (f32[2]{0:T(128)}, f32[2]{0:T(128)S(1)}, u32[]{:S(2)}) copy-start(f32[2]{0:T(128)S(1)} %get-tuple-element.254) | copy-start | bytes 28
  127.8 16.3 %copy-start.16 = (f32[2]{0:T(128)}, f32[2]{0:T(128)S(1)}, u32[]{:S(2)}) copy-start(f32[2]{0:T(128)S(1)} %get-tuple-element.255) | copy-start | bytes 28
  128.3 2.7 copy-start.8
  128.3 2.7 copy-start.9
  128.3 15.9 %copy-start.13 = (f32[2]{0:T(128)}, f32[2]{0:T(128)S(1)}, u32[]{:S(2)}) copy-start(f32[2]{0:T(128)S(1)} %get-tuple-element.295) | copy-start | bytes 28
  129.6 1.4 copy-start.17
  129.7 1.1 copy-start.18
  129.8 1.0 copy-start.19
  163.3 17.9 %copy-start.2 = (pred[128,256]{0,1:T(8,128)(4,1)S(1)}, pred[128,256]{0,1:T(8,128)(4,1)}, u32[]{:S(2)}) copy-start(pred[128,256]{0,1:T(8,128)(4,1)} %fusion.63) | copy-start | bytes 98308
  163.3 17.8 %copy-start.20 = (s32[6]{0:T(128)S(1)}, s32[6]{0:T(128)}, u32[]{:S(2)}) copy-start(s32[6]{0:T(128)} %add_add_fusion) | copy-start | bytes 76
  180.1 4.2 %copy-start.23 = (f32[8]{0:T(128)S(1)}, f32[8]{0:T(128)}, u32[]{:S(2)}) copy-start(f32[8]{0:T(128)} %param.28) | copy-start | bytes 100
  190.7 7.3 %all-to-all-start.3 = ((f32[2,384,4]{1,2,0:T(4,128)}), f32[2,384,4]{1,2,0:T(4,128)}, u32[]{:S(2)}, u32[]{:S(2)}) async-start(f32[2,384,4]{1,2,0:T(4,128)} %bitcast.100), calls=%async_computation.3 | async-start | bytes 24576 | tf_op jit(solution)/shard_map/all_to_all | solution.py:510
  195.6 2.3 copy-start.1
  200.4 59.9 %all-to-all-start.1 = ((bf16[8,768,384]{1,2,0:T(8,128)(2,1)}), bf16[8,768,384]{1,2,0:T(8,128)(2,1)}, u32[]{:S(2)}, u32[]{:S(2)}) async-start(bf16[8,768,384]{1,2,0:T(8,128)(2,1)} %broadcast_in_dim.40), calls=%async_computation.1 | async-start | bytes 9437184 | tf_op jit(solution)/shard_map/all_to_all | solution.py:354
  262.4 2.4 copy-start.21

commit v2 on v1

v2 whole, which is shorter than its diff:
```python
import functools
import math

import jax
import jax.numpy as jnp
from jax import lax
from jax.experimental import pallas as pl
from jax.experimental.pallas import tpu as pltpu
from jax.sharding import Mesh
from jax.sharding import PartitionSpec as P

HD = 64
WINDOW = 128
BLK = 128
EPSILON = 1e-06
MASKED = -1e30
MESH = pl.DeviceIdType.MESH
RING = 4
TOK = 96
ROWS = 8 * TOK
D = 4096
PLANE = ("z", "y")
MAX_COPIES = 200
HALF = ROWS // 2
BLOCKS = ROWS // BLK
CHIPS = RING * RING


class Wires:
    def __init__(self, send_sem, recv_sem):
        self.send_sem, self.recv_sem = send_sem, recv_sem
        self.count = 0
        self.started = []
        z, y, c, x = (lax.axis_index(a) for a in ("z", "y", "c", "x"))
        self.at = {"z": z, "y": y, "c": c, "x": x}

    def moved(self, **new):
        where = dict(self.at)
        where.update(new)
        return (where["z"], where["y"], where["c"], where["x"])

    def step(self, axis, distance):
        return lax.rem(self.at[axis] + distance + RING, RING)

    def neighbour(self, axis, distance):
        return self.moved(**{axis: self.step(axis, distance)})

    def partner(self):
        return self.moved(c=1 - self.at["c"])

    def send(self, src, dst, device):
        k = self.count
        self.count += 1
        copy = pltpu.make_async_remote_copy(
            src_ref=src,
            dst_ref=dst,
            send_sem=self.send_sem.at[k],
            recv_sem=self.recv_sem.at[k],
            device_id=device,
            device_id_type=MESH,
        )
        copy.start()
        self.started.append(copy)
        return k

    def arrived(self, k, dst):
        pltpu.make_async_remote_copy(
            src_ref=dst,
            dst_ref=dst,
            send_sem=self.send_sem.at[k],
            recv_sem=self.recv_sem.at[k],
            device_id=self.partner(),
            device_id_type=MESH,
        ).wait_recv()

    def finish(self):
        for copy in self.started:
            copy.wait_send()


class PlaneGather:
    def __init__(self, wires, whole, depth, core):
        self.w, self.whole, self.depth, self.core = wires, whole, depth, core
        self.first, self.second = ("z", "y") if core == 0 else ("y", "z")
        self.sent = {}

    def rows(self, d1, d2, part=None):
        i1, i2 = self.w.step(self.first, d1), self.w.step(self.second, d2)
        z, y = (i1, i2) if self.core == 0 else (i2, i1)
        start = ((z * RING + y) * 2 + self.core) * self.depth
        half = self.depth // 2
        if part is None:
            return self.whole.at[pl.ds(pl.multiple_of(start, 16), self.depth)]
        return self.whole.at[pl.ds(pl.multiple_of(start + part * half, 16), half)]

    def go(self, name, d1, d2, axis, distance, part=None):
        block = self.rows(d1, d2, part)
        self.sent[name] = self.w.send(block, block, self.w.neighbour(axis, distance))

    def came(self, name, d1, d2, part=None):
        self.w.arrived(self.sent[name], self.rows(d1, d2, part))

    def second_round(self, d1):
        self.go(("b+", d1), d1, 0, self.second, 1)
        self.go(("b-", d1), d1, 0, self.second, -1)

    def start_first(self):
        self.go("a+", 0, 0, self.first, 1)
        self.go("a-", 0, 0, self.first, -1)

    def start_second(self):
        self.second_round(0)

    def first_came(self):
        self.came("a+", -1, 0)
        self.go("ah+", -1, 0, self.first, 1, 0)
        self.second_round(-1)
        self.came("a-", 1, 0)
        self.go("ah-", 1, 0, self.first, -1, 1)
        self.second_round(1)

    def second_came(self, d1):
        self.came(("b+", d1), d1, -1)
        self.go(("bh+", d1), d1, -1, self.second, 1, 0)
        self.came(("b-", d1), d1, 1)
        self.go(("bh-", d1), d1, 1, self.second, -1, 1)

    def first_done(self):
        self.came("ah+", 2, 0, 0)
        self.came("ah-", 2, 0, 1)
        self.second_round(2)

    def second_done(self, d1):
        self.came(("bh+", d1), d1, 2, 0)
        self.came(("bh-", d1), d1, 2, 1)


def plane_steps(wires, whole, depth):
    pair = [PlaneGather(wires, whole, depth, core) for core in (0, 1)]
    steps = []
    for name in ("start_first", "start_second", "first_came"):
        steps += [functools.partial(getattr(g, name)) for g in pair]
    steps += [functools.partial(g.second_came, 0) for g in pair]
    steps += [g.first_done for g in pair]
    for d1 in (-1, 1, 2):
        steps += [functools.partial(g.second_came, d1) for g in pair]
    for d1 in (0, -1, 1, 2):
        steps += [functools.partial(g.second_done, d1) for g in pair]
    return steps


class RowGather:
    def __init__(self, wires, region):
        self.w, self.region = wires, region

    def piece(self, dx, other=False, part=None):
        c = self.w.at["c"]
        return self.region(self.w.step("x", dx), 1 - c if other else c, part)

    def start(self):
        own, w = self.piece(0), self.w
        self.right = w.send(own, own, w.neighbour("x", 1))
        self.left = w.send(own, own, w.neighbour("x", -1))
        self.over = {0: w.send(own, own, w.partner())}

    def came(self):
        w = self.w
        block, half = self.piece(-1), self.piece(-1, part=0)
        w.arrived(self.right, block)
        self.right2 = w.send(half, half, w.neighbour("x", 1))
        self.over[-1] = w.send(block, block, w.partner())
        block, half = self.piece(1), self.piece(1, part=1)
        w.arrived(self.left, block)
        self.left2 = w.send(half, half, w.neighbour("x", -1))
        self.over[1] = w.send(block, block, w.partner())

    def done(self):
        w = self.w
        w.arrived(self.right2, self.piece(2, part=0))
        w.arrived(self.left2, self.piece(2, part=1))
        block = self.piece(2)
        self.over[2] = w.send(block, block, w.partner())

    def shared(self):
        for dx in (0, -1, 1, 2):
            self.w.arrived(self.over[dx], self.piece(dx, other=True))


def dot(a, b, dims=((1,), (0,))):
    return lax.dot_general(a, b, (dims, ((), ())), preferred_element_type=jnp.float32)


def by_head(lane, first, second):
    return jnp.where(lane < HD, first, second)


def joined(one, two):
    passed_one, state_one, normal_one, level_one = one
    passed_two, state_two, normal_two, level_two = two
    level = jnp.maximum(passed_two + level_one, level_two)
    weight_one = jnp.exp(passed_two + level_one - level)
    weight_two = jnp.exp(level_two - level)
    return (
        passed_one + passed_two,
        weight_one * state_one + weight_two * state_two,
        weight_one * normal_one + weight_two * normal_two,
        level,
    )


def put_state(ref, state):
    ref[0:HD, :] = state[1]
    ref[HD : HD + 1, :] = state[2]
    ref[HD + 1 : HD + 2, :] = state[3]
    ref[HD + 2 : HD + 3, :] = state[0]


def get_state(ref):
    return (
        ref[HD + 2 : HD + 3, :], ref[0:HD, :], ref[HD : HD + 1, :], ref[HD + 1 : HD + 2, :]
    )


def layer_kernel(
    tok, gain, wq, wk, wv, wmq, wmk, wmv, wmg, wo, wg, sinks, fbias, fshift,
    out, lt_out,
    tokv, rawkv, kvp, normed, w1, w2, w3, wgv, p1, gate, p2, kd, vd, sh, msgs, pre, outs, lt, ltin,
    stage, rows_in, rows_f, rows_sh, square, send_sem, recv_sem, local_sem,
):
    bf, f32 = jnp.bfloat16, jnp.float32
    w = Wires(send_sem, recv_sem)
    z, y, c, x = (w.at[a] for a in ("z", "y", "c", "x"))
    chip = z * RING + y
    barrier = pltpu.get_barrier_semaphore()
    plane = [(dz, dy) for dz in range(RING) for dy in range(RING) if dz or dy]
    greeted = [w.moved(z=w.step("z", dz), y=w.step("y", dy)) for dz, dy in plane]
    greeted += [w.neighbour("x", 1), w.neighbour("x", -1), w.partner()]
    for device in greeted:
        pl.semaphore_signal(barrier, inc=1, device_id=device, device_id_type=MESH)

    local = []

    def fetch(src, dst):
        copy = pltpu.make_async_copy(src, dst, local_sem.at[len(local)])
        copy.start()
        local.append(copy)
        return copy

    token_copy = fetch(tok, tokv)
    k_copy, v_copy = fetch(wk, rawkv.at[0]), fetch(wv, rawkv.at[1])

    def block_rows(ref, core, depth, cols):
        start = pl.multiple_of(((z * RING + y) * 2 + core) * depth, 16)
        return ref.at[pl.ds(start, depth), cols]

    def cut(ref, width):
        return lambda h: ref.at[:, pl.ds(pl.multiple_of(h * width, 128), width)]

    pieces = [
        (cut(wmk, 128), w1, 128, slice(0, 128)),
        (cut(wmv, 128), w1, 128, slice(128, 256)),
        (cut(wmq, 128), w1, 128, slice(256, 384)),
        (cut(wmg, 128), w1, 128, slice(384, 512)),
        (cut(wq, 256), w2, 128, slice(0, 256)),
        (lambda h: kvp.at[h], w2, 128, slice(256, 384)),
        (cut(wo, 512), w3, 96, slice(0, 512)),
    ]
    kept = [None] * len(pieces)
    for n, (half_of, dst, depth, cols) in enumerate(pieces):
        if n != 5:
            kept[n] = fetch(half_of(c), block_rows(dst, c, depth, cols))
    gate_copy = fetch(wg, wgv)

    k_copy.wait()
    v_copy.wait()
    kvp[0] = jnp.concatenate([rawkv[0, :, :HD], rawkv[1, :, :HD]], axis=1)
    kvp[1] = jnp.concatenate([rawkv[0, :, HD:], rawkv[1, :, HD:]], axis=1)
    sh[c] = fshift[...]
    token_copy.wait()
    first_row = (c * RING + x) * TOK

    def normalize(i, carry):
        values = tokv[pl.ds(pl.multiple_of(i * 16, 16), 16), :].astype(f32)
        rescale = lax.rsqrt(jnp.mean(values * values, axis=-1, keepdims=True) + EPSILON)
        normed[pl.ds(pl.multiple_of(first_row + i * 16, 16), 16), :] = (
            values * rescale * gain[...]
        ).astype(bf)
        return carry

    lax.fori_loop(0, TOK // 16, normalize, 0)
    kept[5] = fetch(kvp.at[c], block_rows(w2, c, 128, slice(256, 384)))
    pl.semaphore_wait(barrier, len(greeted))

    over = [
        w.send(half_of(1 - c), block_rows(dst, c, depth, cols), w.partner())
        for half_of, dst, depth, cols in pieces
    ]

    def token_rows(xi, ci, part):
        start = (ci * RING + xi) * TOK
        if part is None:
            return normed.at[pl.ds(pl.multiple_of(start, 16), TOK)]
        return normed.at[pl.ds(pl.multiple_of(start + part * (TOK // 2), 16), TOK // 2)]

    tokens = RowGather(w, token_rows)
    tokens.start()
    shift_over = w.send(fshift, sh.at[c], w.partner())

    def ready(first, last):
        for n in range(first, last):
            _, dst, depth, cols = pieces[n]
            kept[n].wait()
            w.arrived(over[n], block_rows(dst, 1 - c, depth, cols))

    groups = [plane_steps(w, w1, 128), plane_steps(w, w2, 128), plane_steps(w, w3, 96)]
    groups[0].insert(0, lambda: ready(0, 4))
    groups[1].insert(0, lambda: ready(4, 6))
    groups[2].insert(0, lambda: ready(6, 7))
    at = [0, 0, 0]

    def pump(group, upto):
        while at[group] < min(upto, len(groups[group])):
            groups[group][at[group]]()
            at[group] += 1

    def first_projection(i, carry):
        rows = pl.ds(pl.multiple_of(i * HALF, HALF), HALF)
        p1[rows, :] = dot(normed[rows, :], w1[...]).astype(bf)
        gate[rows, :] = dot(normed[rows, :], wgv[...])
        return carry

    def second_projection(i, carry):
        rows = pl.ds(pl.multiple_of(i * HALF, HALF), HALF)
        both = dot(normed[rows, :], w2[...])
        p2[rows, :] = both[:, :256].astype(bf)
        kv = both[:, 256:]
        turned = pltpu.roll(kv, HD, 1)
        lane = lax.broadcasted_iota(jnp.int32, kv.shape, 1)
        after = pl.ds(pl.multiple_of(i * HALF + WINDOW, WINDOW), HALF)
        kd[after, :] = by_head(lane, kv, turned).astype(bf)
        vd[after, :] = by_head(lane, turned, kv).astype(bf)
        return carry

    lane1 = lax.broadcasted_iota(jnp.int32, (1, 128), 1)
    lane = lax.broadcasted_iota(jnp.int32, (128, 128), 1)
    row = lax.broadcasted_iota(jnp.int32, (128, 128), 0)
    scale = HD ** (-0.5)
    feature_attn = 512 * x + 256 * c
    feature_mem = 2048 + 256 * x + 128 * c

    def memory_gates():
        rows_in[...] = jnp.zeros_like(rows_in)
        rows_f[...] = jnp.zeros_like(rows_f)
        rows_sh[...] = jnp.zeros_like(rows_sh)
        square[...] = jnp.zeros_like(square)
        w.arrived(shift_over, sh.at[1 - c])
        for b in range(BLOCKS):
            turned = jnp.transpose(gate[b * BLK : (b + 1) * BLK, :])
            rows_in[2 * b : 2 * b + 2, :] = turned[0:2]
            rows_f[2 * b : 2 * b + 2, :] = turned[2:4]
            q, at_col = b // 3, (b % 3) * BLK
            both = sh[q, :, at_col : at_col + BLK]
            rows_sh[2 * b : 2 * b + 2, :] = jnp.where(c == 0, both[0:2], both[2:4])
        head = lax.broadcasted_iota(jnp.int32, (16, 128), 0) % 2
        pre_forget = rows_f[...] + jnp.where(head == 0, fbias[2 * c], fbias[2 * c + 1])
        log_forget = (
            jnp.minimum(pre_forget, 0.0)
            - jnp.log1p(jnp.exp(-jnp.abs(pre_forget)))
            + rows_sh[...]
        )
        upto = (row <= lane).astype(f32)
        cumulative = jnp.dot(
            log_forget, upto, precision=lax.Precision.HIGHEST, preferred_element_type=f32
        )
        a = rows_in[...] - 0.5 * math.log(CHIPS * ROWS) - cumulative
        top = jnp.max(a, axis=1, keepdims=True)
        weights = jnp.exp(a - top)
        square[0:16, :] = cumulative
        square[16:32, :] = weights
        rows_in[...] = a
        rows_f[...] = weights
        columns = jnp.transpose(square[...])
        square[...] = columns
        total = cumulative[:, 127:128]
        state = (
            jnp.zeros((1, 128), f32), jnp.zeros((HD, 128), f32), jnp.zeros((1, 128), f32),
            jnp.full((1, 128), MASKED, f32),
        )
        for b in range(BLOCKS):
            put_state(pre.at[b], state)
            rows = slice(b * BLK, (b + 1) * BLK)
            keys, values = p1[rows, 0:128], p1[rows, 128:256]
            spread = by_head(
                lane, columns[:, 16 + 2 * b : 17 + 2 * b], columns[:, 17 + 2 * b : 18 + 2 * b]
            )
            weighted = (values.astype(f32) * spread).astype(bf)
            both = dot(keys, weighted, ((0,), (0,)))
            outer = by_head(lane[:HD], both[:HD], both[HD:]) * scale
            sums = dot(weights.astype(bf), keys)
            normal = by_head(lane1, sums[2 * b : 2 * b + 1], sums[2 * b + 1 : 2 * b + 2]) * scale
            passed = by_head(lane1, total[2 * b : 2 * b + 1], total[2 * b + 1 : 2 * b + 2])
            peak = by_head(lane1, top[2 * b : 2 * b + 1], top[2 * b + 1 : 2 * b + 2])
            state = joined(state, (passed, outer, normal, passed + peak))
        put_state(msgs.at[chip], state)
        msgs[chip, HD + 3 :, :] = jnp.zeros((5, 128), f32)

    told = []

    def tell_state():
        mine = msgs.at[chip]
        for dz, dy in plane:
            device = w.moved(z=w.step("z", dz), y=w.step("y", dy))
            told.append(w.send(mine, mine, device))

    def incoming_state():
        for k, (dz, dy) in zip(told, plane):
            w.arrived(k, msgs.at[w.step("z", -dz) * RING + w.step("y", -dy)])
        state = (
            jnp.zeros((1, 128), f32), jnp.zeros((HD, 128), f32), jnp.zeros((1, 128), f32),
            jnp.full((1, 128), MASKED, f32),
        )
        for other in range(CHIPS - 1):
            after = joined(state, get_state(msgs.at[other]))
            state = tuple(jnp.where(other < chip, new, old) for new, old in zip(after, state))
        return state

    def memory_block(b, incoming):
        rows = slice(b * BLK, (b + 1) * BLK)
        _, state, normal, level = joined(incoming, get_state(pre.at[b]))
        keys, values, query = p1[rows, 0:128], p1[rows, 128:256], p1[rows, 256:384]
        whole = jnp.concatenate(
            [jnp.where(lane[:HD] < HD, state, 0.0), jnp.where(lane[:HD] >= HD, state, 0.0)], axis=0
        ).astype(bf)
        carried_num = dot(query, whole)
        with_normal = query.astype(f32) * normal
        recalled = []
        for h in range(2):
            mine = (lane < HD) if h == 0 else (lane >= HD)
            r = 2 * b + h
            a = jnp.where(row >= lane, rows_in[r : r + 1, :], MASKED)
            stab = level[:, 64 * h : 64 * h + 1]
            high = jnp.maximum(jnp.max(a, axis=1, keepdims=True), stab)
            carried = jnp.exp(stab - high)
            query_h = jnp.where(mine, query, jnp.zeros_like(query))
            affinity = dot(query_h, keys, ((1,), (1,))) * scale * jnp.exp(a - high)
            den = carried * jnp.sum(jnp.where(mine, with_normal, 0.0), axis=1, keepdims=True)
            den = den + jnp.sum(affinity, axis=1, keepdims=True)
            num = carried * carried_num + dot(affinity.astype(bf), values)
            floor = jnp.exp(-(square[:, r : r + 1] + high))
            recalled.append(num / jnp.maximum(jnp.abs(den), floor))
        recall = by_head(lane, recalled[0], recalled[1])
        opened = 1.0 / (1.0 + jnp.exp(-p1[rows, 384:512].astype(f32)))
        outs[rows, pl.ds(pl.multiple_of(feature_mem, 128), 128)] = (recall * opened).astype(bf)

    def attention(first, last):
        query_index = lax.broadcasted_iota(jnp.int32, (WINDOW, 2 * WINDOW), 0)
        key_index = lax.broadcasted_iota(jnp.int32, (WINDOW, 2 * WINDOW), 1)
        distance = query_index - key_index + WINDOW
        in_band = (distance >= 0) & (distance < WINDOW)

        def one_block(b, carry):
            rows = pl.ds(pl.multiple_of(b * WINDOW, WINDOW), WINDOW)
            window = pl.ds(pl.multiple_of(b * WINDOW, WINDOW), 2 * WINDOW)
            keys, values = kd[window, :], vd[window, :]
            allowed = in_band & ((chip * BLOCKS + b) * WINDOW - WINDOW + key_index >= 0)
            logs = jnp.zeros((WINDOW, 128), f32)
            for pair in range(2):
                query = p2[rows, pair * 128 : (pair + 1) * 128]
                results = []
                for half in range(2):
                    h = 2 * pair + half
                    mine = (lane < HD) if half == 0 else (lane >= HD)
                    query_h = jnp.where(mine, query, jnp.zeros_like(query))
                    scores = dot(query_h, keys, ((1,), (1,))) * scale
                    scores = jnp.where(allowed, scores, MASKED)
                    sink = sinks[4 * c + h]
                    ceiling = jnp.maximum(jnp.max(scores, axis=1, keepdims=True), sink)
                    weights = jnp.exp(scores - ceiling)
                    part = jnp.exp(sink - ceiling) + jnp.sum(weights, axis=1, keepdims=True)
                    logs = jnp.where(lane == 4 * c + h, ceiling + jnp.log(part), logs)
                    probs = (weights * (1.0 / part)).astype(bf)
                    results.append(dot(probs, values))
                col = pl.multiple_of(feature_attn + pair * 128, 128)
                outs[rows, pl.ds(col, 128)] = by_head(lane, results[0], results[1]).astype(bf)
            lt[rows, :] = logs
            return carry

        lax.fori_loop(first, last, one_block, 0)

    def out_region(start, base, stride, width):
        def region(xi, ci, part):
            count = HALF if part is None else HALF // 2
            first = start if part is None else start + part * (HALF // 2)
            col = pl.multiple_of(base + 2 * stride * xi + stride * ci, 128)
            return outs.at[pl.ds(first, count), pl.ds(col, width)]

        return RowGather(w, region)

    mem_out = [out_region(r, 2048, 128, 128) for r in (0, HALF)]
    attn_out = [out_region(r, 0, 256, 256) for r in (0, HALF)]

    pump(0, 9)
    pump(1, 5)
    pump(0, 17)
    tokens.came()
    pump(0, 99)
    pump(2, 5)
    pump(1, 9)
    tokens.done()
    tokens.shared()
    gate_copy.wait()
    lax.fori_loop(0, 2, first_projection, 0)
    pump(1, 11)
    memory_gates()
    tell_state()
    pump(1, 17)
    pump(2, 9)
    incoming = incoming_state()
    for b in range(3):
        memory_block(b, incoming)
    mem_out[0].start()
    pump(1, 99)
    for b in range(3, 6):
        memory_block(b, incoming)
    mem_out[1].start()
    lax.fori_loop(0, 2, second_projection, 0)
    next_chip = w.moved(z=lax.rem(z + (y + 1) // RING, RING), y=w.step("y", 1))
    rim = [
        w.send(ref.at[ROWS : ROWS + WINDOW], ref.at[0:WINDOW], next_chip) for ref in (kd, vd)
    ]
    mem_out[0].came()
    pump(2, 13)
    w.arrived(rim[0], kd.at[0:WINDOW])
    w.arrived(rim[1], vd.at[0:WINDOW])
    attention(0, 3)
    attn_out[0].start()
    mem_out[1].came()
    pump(2, 17)
    attention(3, 6)
    attn_out[1].start()
    theirs = pl.ds(pl.multiple_of((1 - c) * HALF, HALF), HALF)
    ours = pl.ds(pl.multiple_of(c * HALF, HALF), HALF)
    log_over = w.send(lt.at[theirs], ltin, w.partner())
    for g in mem_out:
        g.done()
    pump(2, 99)
    for g in attn_out:
        g.came()
    for g in attn_out:
        g.done()
    for g in mem_out + attn_out:
        g.shared()
    stage[...] = dot(outs[theirs, :], w3[...]).astype(bf)
    mixed_over = w.send(stage, out.at[:, pl.ds(pl.multiple_of(c * 512, 512), 512)], w.partner())
    out[:, pl.ds(pl.multiple_of(c * 512, 512), 512)] = dot(outs[ours, :], w3[...]).astype(bf)
    w.arrived(log_over, ltin)
    lt_out[...] = (lt[ours, :] + ltin[...])[:, :8]
    w.arrived(mixed_over, out.at[:, pl.ds(pl.multiple_of((1 - c) * 512, 512), 512)])
    w.finish()


def shards(
    tokens, norm_gain, w_query, w_key, w_value, w_mem_query, w_mem_key, w_mem_value, w_mem_gate,
    w_gates, sinks, forget_bias, forget_shift, w_out,
):
    c, x = lax.axis_index("c"), lax.axis_index("x")
    gates = lax.dynamic_slice_in_dim(w_gates, x * 4 + c * 2, 2, 2).reshape(D, 4)
    gates = jnp.pad(gates, ((0, 0), (0, 124)))
    vmem = pl.BlockSpec(memory_space=pltpu.VMEM)
    smem = pl.BlockSpec(memory_space=pltpu.SMEM)
    anywhere = pl.BlockSpec(memory_space=pl.ANY)
    bf, f32 = jnp.bfloat16, jnp.float32
    mixed, log_total = pl.pallas_call(
        layer_kernel,
        out_shape=[
            jax.ShapeDtypeStruct((HALF, 1024), bf),
            jax.ShapeDtypeStruct((HALF, 8), f32),
        ],
        in_specs=[anywhere, vmem] + [anywhere] * 9 + [smem, smem, vmem],
        out_specs=[vmem, vmem],
        scratch_shapes=[
            pltpu.VMEM((TOK, D), bf),
            pltpu.VMEM((2, 128, 128), bf),
            pltpu.VMEM((2, 128, 128), bf),
            pltpu.VMEM((ROWS, D), bf),
            pltpu.VMEM((D, 512), bf),
            pltpu.VMEM((D, 384), bf),
            pltpu.VMEM((3072, 512), bf),
            pltpu.VMEM((D, 128), bf),
            pltpu.VMEM((ROWS, 512), bf),
            pltpu.VMEM((ROWS, 128), f32),
            pltpu.VMEM((ROWS, 256), bf),
            pltpu.VMEM((ROWS + WINDOW, 128), bf),
            pltpu.VMEM((ROWS + WINDOW, 128), bf),
            pltpu.VMEM((2, 4, HALF), f32),
            pltpu.VMEM((CHIPS, HD + 8, 128), f32),
            pltpu.VMEM((BLOCKS, HD + 8, 128), f32),
            pltpu.VMEM((ROWS, 3072), bf),
            pltpu.VMEM((ROWS, 128), f32),
            pltpu.VMEM((HALF, 128), f32),
            pltpu.VMEM((HALF, 512), bf),
            pltpu.VMEM((16, 128), f32),
            pltpu.VMEM((16, 128), f32),
            pltpu.VMEM((16, 128), f32),
            pltpu.VMEM((128, 128), f32),
            pltpu.SemaphoreType.DMA((MAX_COPIES,)),
            pltpu.SemaphoreType.DMA((MAX_COPIES,)),
            pltpu.SemaphoreType.DMA((16,)),
        ],
        compiler_params=pltpu.CompilerParams(
            collective_id=0, has_side_effects=True, vmem_limit_bytes=60 * 1024 * 1024
        ),
        name="layer",
    )(
        tokens, norm_gain.reshape(1, D), w_query, w_key, w_value, w_mem_query, w_mem_key,
        w_mem_value, w_mem_gate, w_out, gates, sinks, forget_bias, forget_shift.T,
    )
    return (mixed, log_total)


def solution(mesh):
    torus = Mesh(mesh.devices.reshape(4, 4, 2, mesh.shape["tp"]), ("z", "y", "c", "x"))
    sp = ("z", "y", "c")
    placed = (
        (P(("z", "y", "c", "x"), None), P())
        + (P(sp, "x"),) * 7
        + (P(), P("x"), P("x"), P(sp, "x"), P(sp, "x"))
    )
    return jax.shard_map(
        shards, mesh=torus, in_specs=placed, out_specs=(P(sp, "x"), P(sp, "x")), check_vma=False
    )
```

time: 275 us -> 114 us (0.41)
  waiting for transfers between devices: 54 us -> 0 us
  matrix products: 36.3 us -> 0 us
  blocking collectives: 29.4 us -> 0 us
  Pallas kernels: 82.3 us -> 105 us
  local copies, waits for them, and re-layouts: 28.9 us -> 6.39 us
  other arithmetic: 22.5 us -> 0 us
  starting transfers between devices: 17.5 us -> 0 us
    all_to_all x3 -> x0, waiting for transfers between devices: 54 us -> none  [the longest x1 53.9 us: from_everyone(): return lax.all_to_all(copies, axis, split_axis=0, concat_axis=0, tiled=True)]
    dot_general x54 -> x0, matrix products: 36.3 us -> none  [the longest x1 7.47 us: shards(): jnp.dot(normed, w2, preferred_element_type=jnp.float32).astype(jnp.bfloat16)]
    all_gather x2 -> x0, blocking collectives: 25.1 us -> none  [collected_together(): both, at, found = (lax.all_gather(jnp.concatenate(lines), axis), 0, {})]
    pallas_call x1, Pallas kernels: 82.3 us -> 105 us  [shards(): pl.pallas_call(layer_kernel, out_shape=[jax.ShapeDtypeStruct((HALF, 1024)...]
    all_to_all x3 -> x0, starting transfers between devices: 11.6 us -> none  [the longest x2 7.04 us: swapped(): return lax.all_to_all(x, 'c', split_axis=0, concat_axis=0, tiled=True)]
    slice x29 -> x0, local copies, waits for them, and re-layouts: 9.84 us -> none  [the longest x12 2.23 us: advance(): block_total = cumulative[:, -1]]
    ppermute x2 -> x0, starting transfers between devices: 5.82 us -> none  [passed_along(): return lax.ppermute(block, axis, route)]
    convert_element_type x11 -> x0, local copies, waits for them, and re-layouts: 5.02 us -> none  [the longest x8 4.52 us: entering(): part[k].astype(own.dtype)]
  transfers between devices with their start and end apart: 5 -> 0, of which waited for: 1 -> 0; matrix products, arithmetic and copies ran while one was open for 23% -> 0% of each run, Pallas kernels for 0% -> 0%
where the time goes in v2:
time: 114 us; the launch traced here: 112 us
  Pallas kernels  105 us (92%)
  local copies, waits for them, and re-layouts  6.39 us (6%)
    pallas_call x1, Pallas kernels, shards(): pl.pallas_call(layer_kernel, out_shape=[jax.ShapeDtypeStruct((HALF, 1024)...  105 us
    unnamed x3, local copies, waits for them, and re-layouts  3 us

profile of v2, /device:TPU:0, one launch (start us, length us, event | category | flops | bytes accessed | tf_op | source)
XLA Modules:
  0.0 112.1 jit_solution(704133356824551793)
XLA Ops:
  0.6 0.0 copy-start
  0.7 0.9 copy-done
  1.7 0.5 copy.18
  2.2 1.2 %pad.4.wg = bf16[4096,128]{1,0:T(8,128)(2,1)} pad(bf16[4096,4]{1,0:T(8,128)(2,1)S(1)} %copy.18, bf16[]{:T(256)} %constant.18.clone.1), padding=0_0x0_124 | pad | bytes 1081346 | tf_op jit(solution)/shard_map/jit(_pad)/pad | solution.py:568
  3.4 105.1 %layer.1 = (bf16[384,1024]{1,0:T(8,128)(2,1)}, f32[384,8]{1,0:T(8,128)}) custom-call(bf16[96,4096]{1,0:T(8,128)(2,1)} %tok.1, f32[1,4096]{1,0:T(1,128)} %bitcast.4, bf16[128,512]{1,0:T(8,128)(2,1)} %wq.1, bf16[128,128]{1,0:T(8,128)(2,1)} %wk.1, bf16[128,128]{1,0:T(8,128)(2,1)} %wv.1, bf16[128,256]{1,0:T(8,128)(2,1)} %wmq.1, bf16[128,256]{1,0:T(8,128)(2,1)} %wmk.1, ...), custom_call_target="tpu_custom_call" | custom-call | tf_op jit(solution)/shard_map/layer/pallas_call | solution.py:573
  108.4 1.6 %copy.19 = f32[384,8]{0,1:T(8,128)} copy(f32[384,8]{1,0:T(8,128)} %get-tuple-element.5) | data formatting | bytes 24576 | tf_op jit(solution)/shard_map/layer/pallas_call | solution.py:573
  110.1 2.1 %copy.21 = bf16[384,1024]{1,0:T(8,128)(2,1)} copy(bf16[384,1024]{1,0:T(8,128)(2,1)} %get-tuple-element.8) | data formatting | bytes 1572864
  (2 shorter events, 0.1 us)
Async XLA Ops:
  0.6 1.0 copy-start

commit v3 on v2

--- a/solution.py
+++ b/solution.py
@@ -1,5 +1,6 @@
 import functools
 import math
+import types
 
 import jax
 import jax.numpy as jnp
@@ -20,7 +21,7 @@
 ROWS = 8 * TOK
 D = 4096
 PLANE = ("z", "y")
-MAX_COPIES = 200
+MAX_COPIES = 208
 HALF = ROWS // 2
 BLOCKS = ROWS // BLK
 CHIPS = RING * RING
@@ -33,6 +34,7 @@
         self.started = []
         z, y, c, x = (lax.axis_index(a) for a in ("z", "y", "c", "x"))
         self.at = {"z": z, "y": y, "c": c, "x": x}
+        self.steps = {}
 
     def moved(self, **new):
         where = dict(self.at)
@@ -40,7 +42,12 @@
         return (where["z"], where["y"], where["c"], where["x"])
 
     def step(self, axis, distance):
-        return lax.rem(self.at[axis] + distance + RING, RING)
+        if distance % RING == 0:
+            return self.at[axis]
+        key = (axis, distance % RING)
+        if key not in self.steps:
+            self.steps[key] = lax.rem(self.at[axis] + key[1], RING)
+        return self.steps[key]
 
     def neighbour(self, axis, distance):
         return self.moved(**{axis: self.step(axis, distance)})
@@ -81,71 +88,68 @@
 class PlaneGather:
     def __init__(self, wires, whole, depth, core):
         self.w, self.whole, self.depth, self.core = wires, whole, depth, core
-        self.first, self.second = ("z", "y") if core == 0 else ("y", "z")
         self.sent = {}
 
+    def mixed(self, axis, one, two):
+        first, second = (one, two) if axis == "z" else (two, one)
+        return self.w.step(axis, first) * (1 - self.core) + self.w.step(axis, second) * self.core
+
     def rows(self, d1, d2, part=None):
-        i1, i2 = self.w.step(self.first, d1), self.w.step(self.second, d2)
-        z, y = (i1, i2) if self.core == 0 else (i2, i1)
+        z, y = self.mixed("z", d1, d2), self.mixed("y", d1, d2)
         start = ((z * RING + y) * 2 + self.core) * self.depth
         half = self.depth // 2
         if part is None:
             return self.whole.at[pl.ds(pl.multiple_of(start, 16), self.depth)]
         return self.whole.at[pl.ds(pl.multiple_of(start + part * half, 16), half)]
 
-    def go(self, name, d1, d2, axis, distance, part=None):
+    def go(self, name, d1, d2, first, distance, part=None):
         block = self.rows(d1, d2, part)
-        self.sent[name] = self.w.send(block, block, self.w.neighbour(axis, distance))
+        one, two = (distance, 0) if first else (0, distance)
+        device = self.w.moved(z=self.mixed("z", one, two), y=self.mixed("y", one, two))
+        self.sent[name] = self.w.send(block, block, device)
 
     def came(self, name, d1, d2, part=None):
         self.w.arrived(self.sent[name], self.rows(d1, d2, part))
 
     def second_round(self, d1):
-        self.go(("b+", d1), d1, 0, self.second, 1)
-        self.go(("b-", d1), d1, 0, self.second, -1)
-
-    def start_first(self):
-        self.go("a+", 0, 0, self.first, 1)
-        self.go("a-", 0, 0, self.first, -1)
-
-    def start_second(self):
+        self.go(("b", 1, d1), d1, 0, False, 1)
+        self.go(("b", -1, d1), d1, 0, False, -1)
+
+    def start(self):
+        self.go(("a", 1), 0, 0, True, 1)
+        self.go(("a", -1), 0, 0, True, -1)
         self.second_round(0)
 
-    def first_came(self):
-        self.came("a+", -1, 0)
-        self.go("ah+", -1, 0, self.first, 1, 0)
-        self.second_round(-1)
-        self.came("a-", 1, 0)
-        self.go("ah-", 1, 0, self.first, -1, 1)
-        self.second_round(1)
-
-    def second_came(self, d1):
-        self.came(("b+", d1), d1, -1)
-        self.go(("bh+", d1), d1, -1, self.second, 1, 0)
-        self.came(("b-", d1), d1, 1)
-        self.go(("bh-", d1), d1, 1, self.second, -1, 1)
-
-    def first_done(self):
-        self.came("ah+", 2, 0, 0)
-        self.came("ah-", 2, 0, 1)
-        self.second_round(2)
-
-    def second_done(self, d1):
-        self.came(("bh+", d1), d1, 2, 0)
-        self.came(("bh-", d1), d1, 2, 1)
-
-
-def plane_steps(wires, whole, depth):
-    pair = [PlaneGather(wires, whole, depth, core) for core in (0, 1)]
-    steps = []
-    for name in ("start_first", "start_second", "first_came"):
-        steps += [functools.partial(getattr(g, name)) for g in pair]
-    steps += [functools.partial(g.second_came, 0) for g in pair]
-    steps += [g.first_done for g in pair]
+    def first_came(self, side):
+        self.came(("a", side), -side, 0)
+        self.go(("ah", side), -side, 0, True, side, 0 if side > 0 else 1)
+        self.second_round(-side)
+
+    def second_came(self, d1, side):
+        self.came(("b", side, d1), d1, -side)
+        self.go(("bh", side, d1), d1, -side, False, side, 0 if side > 0 else 1)
+
+    def first_done(self, side):
+        self.came(("ah", side), 2, 0, 0 if side > 0 else 1)
+        if side < 0:
+            self.second_round(2)
+
+    def second_done(self, d1, side):
+        self.came(("bh", side, d1), d1, 2, 0 if side > 0 else 1)
+
+
+def plane_steps(wires, whole, depth, own_ready, other_ready):
+    c = wires.at["c"]
+    pair = [PlaneGather(wires, whole, depth, core) for core in (c, 1 - c)]
+    both = [(g, side) for side in (1, -1) for g in pair]
+    steps = [own_ready, pair[0].start, other_ready, pair[1].start]
+    steps += [functools.partial(g.first_came, side) for g, side in both]
+    steps += [functools.partial(g.second_came, 0, side) for g, side in both]
+    steps += [functools.partial(g.first_done, side) for g, side in both]
     for d1 in (-1, 1, 2):
-        steps += [functools.partial(g.second_came, d1) for g in pair]
+        steps += [functools.partial(g.second_came, d1, side) for g, side in both]
     for d1 in (0, -1, 1, 2):
-        steps += [functools.partial(g.second_done, d1) for g in pair]
+        steps += [functools.partial(g.second_done, d1, side) for g, side in both]
     return steps
 
 
@@ -162,28 +166,24 @@
         self.right = w.send(own, own, w.neighbour("x", 1))
         self.left = w.send(own, own, w.neighbour("x", -1))
         self.over = {0: w.send(own, own, w.partner())}
-
-    def came(self):
+        self.again = {}
+
+    def came(self, side):
+        w, part = self.w, 0 if side > 0 else 1
+        block, half = self.piece(-side), self.piece(-side, part=part)
+        w.arrived(self.right if side > 0 else self.left, block)
+        self.again[side] = w.send(half, half, w.neighbour("x", side))
+        self.over[-side] = w.send(block, block, w.partner())
+
+    def done(self, side):
         w = self.w
-        block, half = self.piece(-1), self.piece(-1, part=0)
-        w.arrived(self.right, block)
-        self.right2 = w.send(half, half, w.neighbour("x", 1))
-        self.over[-1] = w.send(block, block, w.partner())
-        block, half = self.piece(1), self.piece(1, part=1)
-        w.arrived(self.left, block)
-        self.left2 = w.send(half, half, w.neighbour("x", -1))
-        self.over[1] = w.send(block, block, w.partner())
-
-    def done(self):
-        w = self.w
-        w.arrived(self.right2, self.piece(2, part=0))
-        w.arrived(self.left2, self.piece(2, part=1))
-        block = self.piece(2)
-        self.over[2] = w.send(block, block, w.partner())
-
-    def shared(self):
-        for dx in (0, -1, 1, 2):
-            self.w.arrived(self.over[dx], self.piece(dx, other=True))
+        w.arrived(self.again[side], self.piece(2, part=0 if side > 0 else 1))
+        if side < 0:
+            block = self.piece(2)
+            self.over[2] = w.send(block, block, w.partner())
+
+    def shared(self, dx):
+        self.w.arrived(self.over[dx], self.piece(dx, other=True))
 
 
 def dot(a, b, dims=((1,), (0,))):
@@ -225,7 +225,7 @@
     tok, gain, wq, wk, wv, wmq, wmk, wmv, wmg, wo, wg, sinks, fbias, fshift,
     out, lt_out,
     tokv, rawkv, kvp, normed, w1, w2, w3, wgv, p1, gate, p2, kd, vd, sh, msgs, pre, outs, lt, ltin,
-    stage, rows_in, rows_f, rows_sh, square, send_sem, recv_sem, local_sem,
+    stage, total, turned, small, rows_in, rows_f, rows_sh, square, send_sem, recv_sem, local_sem,
 ):
     bf, f32 = jnp.bfloat16, jnp.float32
     w = Wires(send_sem, recv_sem)
@@ -233,8 +233,8 @@
     chip = z * RING + y
     barrier = pltpu.get_barrier_semaphore()
     plane = [(dz, dy) for dz in range(RING) for dy in range(RING) if dz or dy]
-    greeted = [w.moved(z=w.step("z", dz), y=w.step("y", dy)) for dz, dy in plane]
-    greeted += [w.neighbour("x", 1), w.neighbour("x", -1), w.partner()]
+    greeted = [w.neighbour(axis, d) for axis in ("z", "y", "x") for d in (1, -1)]
+    greeted.append(w.partner())
     for device in greeted:
         pl.semaphore_signal(barrier, inc=1, device_id=device, device_id_type=MESH)
 
@@ -246,8 +246,8 @@
         local.append(copy)
         return copy
 
+    k_copy, v_copy = fetch(wk, rawkv.at[0]), fetch(wv, rawkv.at[1])
     token_copy = fetch(tok, tokv)
-    k_copy, v_copy = fetch(wk, rawkv.at[0]), fetch(wv, rawkv.at[1])
 
     def block_rows(ref, core, depth, cols):
         start = pl.multiple_of(((z * RING + y) * 2 + core) * depth, 16)
@@ -257,17 +257,17 @@
         return lambda h: ref.at[:, pl.ds(pl.multiple_of(h * width, 128), width)]
 
     pieces = [
-        (cut(wmk, 128), w1, 128, slice(0, 128)),
-        (cut(wmv, 128), w1, 128, slice(128, 256)),
-        (cut(wmq, 128), w1, 128, slice(256, 384)),
-        (cut(wmg, 128), w1, 128, slice(384, 512)),
-        (cut(wq, 256), w2, 128, slice(0, 256)),
-        (lambda h: kvp.at[h], w2, 128, slice(256, 384)),
+        (cut(wq, 256), w1, 128, slice(0, 256)),
+        (lambda h: kvp.at[h], w1, 128, slice(256, 384)),
+        (cut(wmk, 128), w1, 128, slice(384, 512)),
+        (cut(wmv, 128), w1, 128, slice(512, 640)),
+        (cut(wmq, 128), w2, 128, slice(0, 128)),
+        (cut(wmg, 128), w2, 128, slice(128, 256)),
         (cut(wo, 512), w3, 96, slice(0, 512)),
     ]
     kept = [None] * len(pieces)
     for n, (half_of, dst, depth, cols) in enumerate(pieces):
-        if n != 5:
+        if n != 1:
             kept[n] = fetch(half_of(c), block_rows(dst, c, depth, cols))
     gate_copy = fetch(wg, wgv)
 
@@ -276,7 +276,21 @@
     kvp[0] = jnp.concatenate([rawkv[0, :, :HD], rawkv[1, :, :HD]], axis=1)
     kvp[1] = jnp.concatenate([rawkv[0, :, HD:], rawkv[1, :, HD:]], axis=1)
     sh[c] = fshift[...]
-    token_copy.wait()
+    kept[1] = fetch(kvp.at[c], block_rows(w1, c, 128, slice(256, 384)))
+    pl.semaphore_wait(barrier, len(greeted))
+
+    over = [
+        w.send(half_of(1 - c), block_rows(dst, c, depth, cols), w.partner())
+        for half_of, dst, depth, cols in pieces
+    ]
+
+    def token_rows(xi, ci, part):
+        start = (ci * RING + xi) * TOK
+        if part is None:
+            return normed.at[pl.ds(pl.multiple_of(start, 16), TOK)]
+        return normed.at[pl.ds(pl.multiple_of(start + part * (TOK // 2), 16), TOK // 2)]
+
+    tokens = RowGather(w, token_rows)
     first_row = (c * RING + x) * TOK
 
     def normalize(i, carry):
@@ -287,35 +301,24 @@
         ).astype(bf)
         return carry
 
-    lax.fori_loop(0, TOK // 16, normalize, 0)
-    kept[5] = fetch(kvp.at[c], block_rows(w2, c, 128, slice(256, 384)))
-    pl.semaphore_wait(barrier, len(greeted))
-
-    over = [
-        w.send(half_of(1 - c), block_rows(dst, c, depth, cols), w.partner())
-        for half_of, dst, depth, cols in pieces
-    ]
-
-    def token_rows(xi, ci, part):
-        start = (ci * RING + xi) * TOK
-        if part is None:
-            return normed.at[pl.ds(pl.multiple_of(start, 16), TOK)]
-        return normed.at[pl.ds(pl.multiple_of(start + part * (TOK // 2), 16), TOK // 2)]
-
-    tokens = RowGather(w, token_rows)
-    tokens.start()
     shift_over = w.send(fshift, sh.at[c], w.partner())
 
-    def ready(first, last):
+    def own_ready(first, last):
+        for n in range(first, last):
+            kept[n].wait()
+
+    def other_ready(first, last):
         for n in range(first, last):
             _, dst, depth, cols = pieces[n]
-            kept[n].wait()
             w.arrived(over[n], block_rows(dst, 1 - c, depth, cols))
 
-    groups = [plane_steps(w, w1, 128), plane_steps(w, w2, 128), plane_steps(w, w3, 96)]
-    groups[0].insert(0, lambda: ready(0, 4))
-    groups[1].insert(0, lambda: ready(4, 6))
-    groups[2].insert(0, lambda: ready(6, 7))
+    groups = [
+        plane_steps(
+            w, whole, depth,
+            functools.partial(own_ready, *span), functools.partial(other_ready, *span),
+        )
+        for whole, depth, span in ((w1, 128, (0, 4)), (w2, 128, (4, 6)), (w3, 96, (6, 7)))
+    ]
     at = [0, 0, 0]
 
     def pump(group, upto):
@@ -323,23 +326,22 @@
             groups[group][at[group]]()
             at[group] += 1
 
-    def first_projection(i, carry):
-        rows = pl.ds(pl.multiple_of(i * HALF, HALF), HALF)
-        p1[rows, :] = dot(normed[rows, :], w1[...]).astype(bf)
-        gate[rows, :] = dot(normed[rows, :], wgv[...])
-        return carry
-
-    def second_projection(i, carry):
-        rows = pl.ds(pl.multiple_of(i * HALF, HALF), HALF)
-        both = dot(normed[rows, :], w2[...])
+    def first_projection(i):
+        rows = slice(i * HALF, (i + 1) * HALF)
+        both = dot(normed[rows, :], w1[...])
         p2[rows, :] = both[:, :256].astype(bf)
-        kv = both[:, 256:]
-        turned = pltpu.roll(kv, HD, 1)
+        kv = both[:, 256:384]
+        turned_kv = pltpu.roll(kv, HD, 1)
         lane = lax.broadcasted_iota(jnp.int32, kv.shape, 1)
-        after = pl.ds(pl.multiple_of(i * HALF + WINDOW, WINDOW), HALF)
-        kd[after, :] = by_head(lane, kv, turned).astype(bf)
-        vd[after, :] = by_head(lane, turned, kv).astype(bf)
-        return carry
+        after = slice(i * HALF + WINDOW, (i + 1) * HALF + WINDOW)
+        kd[after, :] = by_head(lane, kv, turned_kv).astype(bf)
+        vd[after, :] = by_head(lane, turned_kv, kv).astype(bf)
+        p1[rows, 0:256] = both[:, 384:].astype(bf)
+        gate[rows, 0:32] = dot(normed[rows, :], wgv[...], ((1,), (1,)))
+
+    def second_projection(i):
+        rows = slice(i * HALF, (i + 1) * HALF)
+        p1[rows, 256:512] = dot(normed[rows, :], w2[...]).astype(bf)
 
     lane1 = lax.broadcasted_iota(jnp.int32, (1, 128), 1)
     lane = lax.broadcasted_iota(jnp.int32, (128, 128), 1)
@@ -352,12 +354,15 @@
         rows_in[...] = jnp.zeros_like(rows_in)
         rows_f[...] = jnp.zeros_like(rows_f)
         rows_sh[...] = jnp.zeros_like(rows_sh)
+        gate[:, 32:] = jnp.zeros((ROWS, 96), f32)
         square[...] = jnp.zeros_like(square)
         w.arrived(shift_over, sh.at[1 - c])
         for b in range(BLOCKS):
-            turned = jnp.transpose(gate[b * BLK : (b + 1) * BLK, :])
-            rows_in[2 * b : 2 * b + 2, :] = turned[0:2]
-            rows_f[2 * b : 2 * b + 2, :] = turned[2:4]
+            turned[...] = jnp.transpose(gate[b * BLK : (b + 1) * BLK, :])
+            for h in range(2):
+                own = 4 * x + 2 * c + h
+                rows_in[2 * b + h : 2 * b + h + 1, :] = turned[pl.ds(own, 1), :]
+                rows_f[2 * b + h : 2 * b + h + 1, :] = turned[pl.ds(16 + own, 1), :]
             q, at_col = b // 3, (b % 3) * BLK
             both = sh[q, :, at_col : at_col + BLK]
             rows_sh[2 * b : 2 * b + 2, :] = jnp.where(c == 0, both[0:2], both[2:4])
@@ -381,7 +386,7 @@
         rows_f[...] = weights
         columns = jnp.transpose(square[...])
         square[...] = columns
-        total = cumulative[:, 127:128]
+        ends = cumulative[:, 127:128]
         state = (
             jnp.zeros((1, 128), f32), jnp.zeros((HD, 128), f32), jnp.zeros((1, 128), f32),
             jnp.full((1, 128), MASKED, f32),
@@ -398,11 +403,18 @@
             outer = by_head(lane[:HD], both[:HD], both[HD:]) * scale
             sums = dot(weights.astype(bf), keys)
             normal = by_head(lane1, sums[2 * b : 2 * b + 1], sums[2 * b + 1 : 2 * b + 2]) * scale
-            passed = by_head(lane1, total[2 * b : 2 * b + 1], total[2 * b + 1 : 2 * b + 2])
+            passed = by_head(lane1, ends[2 * b : 2 * b + 1], ends[2 * b + 1 : 2 * b + 2])
             peak = by_head(lane1, top[2 * b : 2 * b + 1], top[2 * b + 1 : 2 * b + 2])
             state = joined(state, (passed, outer, normal, passed + peak))
-        put_state(msgs.at[chip], state)
-        msgs[chip, HD + 3 :, :] = jnp.zeros((5, 128), f32)
+        small[...] = jnp.zeros_like(small)
+        small[0:1, :] = state[2]
+        for first, exact in ((1, state[3]), (4, state[0])):
+            for k in range(3):
+                term = exact.astype(bf).astype(f32)
+                small[first + k : first + k + 1, :] = term
+                exact = exact - term
+        msgs[chip, 0:HD, :] = state[1].astype(bf)
+        msgs[chip, HD : HD + 16, :] = small[...].astype(bf)
 
     told = []
 
@@ -420,7 +432,12 @@
             jnp.full((1, 128), MASKED, f32),
         )
         for other in range(CHIPS - 1):
-            after = joined(state, get_state(msgs.at[other]))
+            rest = msgs[other, HD : HD + 16, :].astype(f32)
+            came = (
+                rest[4:5] + rest[5:6] + rest[6:7], msgs[other, 0:HD, :].astype(f32),
+                rest[0:1], rest[1:2] + rest[2:3] + rest[3:4],
+            )
+            after = joined(state, came)
             state = tuple(jnp.where(other < chip, new, old) for new, old in zip(after, state))
         return state
 
@@ -487,85 +504,196 @@
 
         lax.fori_loop(first, last, one_block, 0)
 
+    third = ROWS // 3
+
     def out_region(start, base, stride, width):
         def region(xi, ci, part):
-            count = HALF if part is None else HALF // 2
-            first = start if part is None else start + part * (HALF // 2)
+            count = third if part is None else third // 2
+            first = start if part is None else start + part * (third // 2)
             col = pl.multiple_of(base + 2 * stride * xi + stride * ci, 128)
             return outs.at[pl.ds(first, count), pl.ds(col, width)]
 
         return RowGather(w, region)
 
-    mem_out = [out_region(r, 2048, 128, 128) for r in (0, HALF)]
-    attn_out = [out_region(r, 0, 256, 256) for r in (0, HALF)]
-
-    pump(0, 9)
-    pump(1, 5)
-    pump(0, 17)
-    tokens.came()
-    pump(0, 99)
-    pump(2, 5)
-    pump(1, 9)
-    tokens.done()
-    tokens.shared()
-    gate_copy.wait()
-    lax.fori_loop(0, 2, first_projection, 0)
-    pump(1, 11)
-    memory_gates()
-    tell_state()
-    pump(1, 17)
-    pump(2, 9)
-    incoming = incoming_state()
-    for b in range(3):
-        memory_block(b, incoming)
-    mem_out[0].start()
-    pump(1, 99)
-    for b in range(3, 6):
-        memory_block(b, incoming)
-    mem_out[1].start()
-    lax.fori_loop(0, 2, second_projection, 0)
-    next_chip = w.moved(z=lax.rem(z + (y + 1) // RING, RING), y=w.step("y", 1))
-    rim = [
-        w.send(ref.at[ROWS : ROWS + WINDOW], ref.at[0:WINDOW], next_chip) for ref in (kd, vd)
-    ]
-    mem_out[0].came()
-    pump(2, 13)
-    w.arrived(rim[0], kd.at[0:WINDOW])
-    w.arrived(rim[1], vd.at[0:WINDOW])
-    attention(0, 3)
-    attn_out[0].start()
-    mem_out[1].came()
-    pump(2, 17)
-    attention(3, 6)
-    attn_out[1].start()
+    mem_out = [out_region(i * third, 2048, 128, 128) for i in range(3)]
+    attn_out = [out_region(i * third, 0, 256, 256) for i in range(3)]
     theirs = pl.ds(pl.multiple_of((1 - c) * HALF, HALF), HALF)
     ours = pl.ds(pl.multiple_of(c * HALF, HALF), HALF)
-    log_over = w.send(lt.at[theirs], ltin, w.partner())
-    for g in mem_out:
-        g.done()
-    pump(2, 99)
-    for g in attn_out:
-        g.came()
-    for g in attn_out:
-        g.done()
-    for g in mem_out + attn_out:
-        g.shared()
-    stage[...] = dot(outs[theirs, :], w3[...]).astype(bf)
-    mixed_over = w.send(stage, out.at[:, pl.ds(pl.multiple_of(c * 512, 512), 512)], w.partner())
-    out[:, pl.ds(pl.multiple_of(c * 512, 512), 512)] = dot(outs[ours, :], w3[...]).astype(bf)
-    w.arrived(log_over, ltin)
-    lt_out[...] = (lt[ours, :] + ltin[...])[:, :8]
-    w.arrived(mixed_over, out.at[:, pl.ds(pl.multiple_of((1 - c) * 512, 512), 512)])
-    w.finish()
+
+    def normalize_all():
+        token_copy.wait()
+        lax.fori_loop(0, TOK // 16, normalize, 0)
+
+    kept_values = {}
+
+    def rim_start():
+        next_chip = w.moved(z=lax.rem(z + (y + 1) // RING, RING), y=w.step("y", 1))
+        kept_values["rim"] = [
+            w.send(ref.at[ROWS : ROWS + WINDOW], ref.at[0:WINDOW], next_chip) for ref in (kd, vd)
+        ]
+
+    def rim_came():
+        w.arrived(kept_values["rim"][0], kd.at[0:WINDOW])
+        w.arrived(kept_values["rim"][1], vd.at[0:WINDOW])
+
+    def state_came():
+        kept_values["state"] = incoming_state()
+
+    def memory_blocks(first, last):
+        for b in range(first, last):
+            memory_block(b, kept_values["state"])
+
+    def out_first(half):
+        rows = (theirs, ours)[half]
+        total[rows, :] = dot(outs[rows, :2048], w3[:2048])
+
+    def log_start():
+        kept_values["log"] = w.send(lt.at[theirs], ltin, w.partner())
+
+    def out_last():
+        out_cols = out.at[:, pl.ds(pl.multiple_of(c * 512, 512), 512)]
+        stage[...] = (total[theirs, :] + dot(outs[theirs, 2048:], w3[2048:])).astype(bf)
+        mixed_over = w.send(stage, out_cols, w.partner())
+        out[:, pl.ds(pl.multiple_of(c * 512, 512), 512)] = (
+            total[ours, :] + dot(outs[ours, 2048:], w3[2048:])
+        ).astype(bf)
+        w.arrived(kept_values["log"], ltin)
+        lt_out[...] = jnp.transpose(lt[ours, :] + ltin[...])[:8]
+        w.arrived(mixed_over, out.at[:, pl.ds(pl.multiple_of((1 - c) * 512, 512), 512)])
+
+    schedule(
+        types.SimpleNamespace(
+            pump=pump, normalize=normalize_all, finish=w.finish, tokens=tokens, gate_weights=gate_copy.wait,
+            first_projection=first_projection, second_projection=second_projection,
+            rim_start=rim_start, rim_came=rim_came, memory_gates=memory_gates,
+            tell_state=tell_state, state_came=state_came, memory_blocks=memory_blocks,
+            attention=attention, attn_out=attn_out, mem_out=mem_out, out_first=out_first,
+            log_start=log_start, out_last=out_last,
+        )
+    )
+
+
+def schedule(s):
+    pump, attn, mem = s.pump, s.attn_out, s.mem_out
+    pump(0, 2)
+    s.normalize()
+    s.tokens.start()
+    pump(0, 21)
+    pump(1, 4)
+    pump(0, 23)
+    s.tokens.came(1)
+    s.tokens.came(-1)
+    pump(0, 35)
+    pump(1, 5)
+    pump(0, 37)
+    pump(1, 11)
+    pump(0, 39)
+    pump(1, 12)
+    s.tokens.done(1)
+    s.tokens.done(-1)
+    s.tokens.shared(0)
+    s.tokens.shared(-1)
+    s.tokens.shared(1)
+    pump(0, 43)
+    pump(1, 13)
+    s.tokens.shared(2)
+    pump(0, 44)
+    s.gate_weights()
+    s.first_projection(0)
+    pump(1, 24)
+    pump(2, 4)
+    s.first_projection(1)
+    pump(1, 32)
+    s.rim_start()
+    s.memory_gates()
+    pump(1, 40)
+    s.tell_state()
+    s.attention(2, 4)
+    attn[1].start()
+    s.attention(4, 6)
+    attn[2].start()
+    pump(2, 12)
+    pump(1, 44)
+    s.second_projection(0)
+    s.rim_came()
+    s.attention(0, 2)
+    attn[0].start()
+    attn[1].came(1)
+    attn[1].came(-1)
+    s.second_projection(1)
+    attn[2].came(1)
+    attn[2].came(-1)
+    s.log_start()
+    pump(2, 13)
+    s.state_came()
+    s.memory_blocks(0, 2)
+    mem[0].start()
+    attn[0].came(1)
+    attn[0].came(-1)
+    s.memory_blocks(2, 4)
+    mem[1].start()
+    pump(2, 15)
+    attn[1].done(1)
+    attn[1].done(-1)
+    attn[1].shared(0)
+    attn[1].shared(-1)
+    attn[1].shared(1)
+    s.memory_blocks(4, 6)
+    mem[2].start()
+    pump(2, 24)
+    attn[1].shared(2)
+    attn[2].done(1)
+    attn[2].done(-1)
+    attn[2].shared(0)
+    attn[2].shared(-1)
+    attn[2].shared(1)
+    mem[0].came(1)
+    mem[0].came(-1)
+    attn[2].shared(2)
+    attn[0].done(1)
+    attn[0].done(-1)
+    attn[0].shared(0)
+    attn[0].shared(-1)
+    attn[0].shared(1)
+    pump(2, 25)
+    attn[0].shared(2)
+    mem[1].came(1)
+    mem[1].came(-1)
+    pump(2, 33)
+    mem[2].came(1)
+    mem[2].came(-1)
+    pump(2, 37)
+    mem[0].done(1)
+    mem[0].done(-1)
+    mem[0].shared(0)
+    mem[0].shared(-1)
+    mem[0].shared(1)
+    pump(2, 41)
+    mem[1].done(1)
+    mem[1].done(-1)
+    mem[1].shared(0)
+    mem[1].shared(-1)
+    mem[1].shared(1)
+    mem[0].shared(2)
+    pump(2, 44)
+    s.out_first(0)
+    mem[1].shared(2)
+    mem[2].done(1)
+    mem[2].done(-1)
+    mem[2].shared(0)
+    mem[2].shared(-1)
+    mem[2].shared(1)
+    s.out_first(1)
+    mem[2].shared(2)
+    s.out_last()
+    s.finish()
 
 
 def shards(
     tokens, norm_gain, w_query, w_key, w_value, w_mem_query, w_mem_key, w_mem_value, w_mem_gate,
     w_gates, sinks, forget_bias, forget_shift, w_out,
 ):
-    c, x = lax.axis_index("c"), lax.axis_index("x")
-    gates = lax.dynamic_slice_in_dim(w_gates, x * 4 + c * 2, 2, 2).reshape(D, 4)
-    gates = jnp.pad(gates, ((0, 0), (0, 124)))
+    gates = w_gates.transpose(1, 2, 0).reshape(32, D)
     vmem = pl.BlockSpec(memory_space=pltpu.VMEM)
     smem = pl.BlockSpec(memory_space=pltpu.SMEM)
     anywhere = pl.BlockSpec(memory_space=pl.ANY)
@@ -574,7 +702,7 @@
         layer_kernel,
         out_shape=[
             jax.ShapeDtypeStruct((HALF, 1024), bf),
-            jax.ShapeDtypeStruct((HALF, 8), f32),
+            jax.ShapeDtypeStruct((8, HALF), f32),
         ],
         in_specs=[anywhere, vmem] + [anywhere] * 9 + [smem, smem, vmem],
         out_specs=[vmem, vmem],
@@ -583,22 +711,25 @@
             pltpu.VMEM((2, 128, 128), bf),
             pltpu.VMEM((2, 128, 128), bf),
             pltpu.VMEM((ROWS, D), bf),
-            pltpu.VMEM((D, 512), bf),
-            pltpu.VMEM((D, 384), bf),
+            pltpu.VMEM((D, 640), bf),
+            pltpu.VMEM((D, 256), bf),
             pltpu.VMEM((3072, 512), bf),
-            pltpu.VMEM((D, 128), bf),
+            pltpu.VMEM((32, D), bf),
             pltpu.VMEM((ROWS, 512), bf),
             pltpu.VMEM((ROWS, 128), f32),
             pltpu.VMEM((ROWS, 256), bf),
             pltpu.VMEM((ROWS + WINDOW, 128), bf),
             pltpu.VMEM((ROWS + WINDOW, 128), bf),
             pltpu.VMEM((2, 4, HALF), f32),
-            pltpu.VMEM((CHIPS, HD + 8, 128), f32),
+            pltpu.VMEM((CHIPS, HD + 16, 128), bf),
             pltpu.VMEM((BLOCKS, HD + 8, 128), f32),
             pltpu.VMEM((ROWS, 3072), bf),
             pltpu.VMEM((ROWS, 128), f32),
             pltpu.VMEM((HALF, 128), f32),
             pltpu.VMEM((HALF, 512), bf),
+            pltpu.VMEM((ROWS, 512), f32),
+            pltpu.VMEM((128, 128), f32),
+            pltpu.VMEM((16, 128), f32),
             pltpu.VMEM((16, 128), f32),
             pltpu.VMEM((16, 128), f32),
             pltpu.VMEM((16, 128), f32),
@@ -615,7 +746,7 @@
         tokens, norm_gain.reshape(1, D), w_query, w_key, w_value, w_mem_query, w_mem_key,
         w_mem_value, w_mem_gate, w_out, gates, sinks, forget_bias, forget_shift.T,
     )
-    return (mixed, log_total)
+    return (mixed, log_total.T)
 
 
 def solution(mesh):

time: 114 us -> 91 us (0.80)
  Pallas kernels: 105 us -> 86.3 us
  local copies, waits for them, and re-layouts: 6.39 us -> 2.67 us
    pallas_call x1, Pallas kernels: 105 us -> 86.3 us  [shards(): pl.pallas_call(layer_kernel, out_shape=[jax.ShapeDtypeStruct((HALF, 1024)...]
    pallas_call x1 -> x0, local copies, waits for them, and re-layouts: 1.63 us -> none  [shards(): pl.pallas_call(layer_kernel, out_shape=[jax.ShapeDtypeStruct((HALF, 1024)...]
    pad x1 -> x0, local copies, waits for them, and re-layouts: 1.18 us -> none  [shards(): gates = jnp.pad(gates, ((0, 0), (0, 124)))]
    unnamed x3 -> x4, local copies, waits for them, and re-layouts: 3 us -> 2.67 us
where the time goes in v3:
time: 91 us; the launch traced here: 89.6 us
  Pallas kernels  86.3 us (95%)
  local copies, waits for them, and re-layouts  2.67 us (3%)
    pallas_call x1, Pallas kernels, shards(): pl.pallas_call(layer_kernel, out_shape=[jax.ShapeDtypeStruct((HALF, 1024)...  86.3 us
    unnamed x4, local copies, waits for them, and re-layouts  2.67 us

profile of v3, /device:TPU:0, one launch (start us, length us, event | category | flops | bytes accessed | tf_op | source)
XLA Modules:
  0.0 89.6 jit_solution(6067894127912989669)
XLA Ops:
  0.6 86.3 %layer.1 = (bf16[384,1024]{1,0:T(8,128)(2,1)}, f32[8,384]{1,0:T(8,128)}) custom-call(bf16[96,4096]{1,0:T(8,128)(2,1)} %tok.1, f32[1,4096]{1,0:T(1,128)} %bitcast.7, bf16[128,512]{1,0:T(8,128)(2,1)} %wq.1, bf16[128,128]{1,0:T(8,128)(2,1)} %wk.1, bf16[128,128]{1,0:T(8,128)(2,1)} %wv.1, bf16[128,256]{1,0:T(8,128)(2,1)} %wmq.1, bf16[128,256]{1,0:T(8,128)(2,1)} %wmk.1, ...), custom_call_target="tpu_custom_call" | custom-call | tf_op jit(solution)/shard_map/layer/pallas_call | solution.py:701
  87.0 0.0 copy-start
  87.0 2.1 %copy.18 = bf16[384,1024]{1,0:T(8,128)(2,1)} copy(bf16[384,1024]{1,0:T(8,128)(2,1)} %get-tuple-element.8) | data formatting | bytes 1572864
  89.0 0.0 copy-done
  89.0 0.6 copy.19
Async XLA Ops:
  87.0 2.1 %copy-start = (f32[8,384]{1,0:T(8,128)S(1)}, f32[8,384]{1,0:T(8,128)}, u32[]{:S(2)}) copy-start(f32[8,384]{1,0:T(8,128)} %get-tuple-element.5) | copy-start | bytes 36868

commit v4 on v3

--- a/solution.py
+++ b/solution.py
@@ -21,7 +21,8 @@
 ROWS = 8 * TOK
 D = 4096
 PLANE = ("z", "y")
-MAX_COPIES = 208
+SENDS = 12
+RECEIVES = 72
 HALF = ROWS // 2
 BLOCKS = ROWS // BLK
 CHIPS = RING * RING
@@ -30,11 +31,9 @@
 class Wires:
     def __init__(self, send_sem, recv_sem):
         self.send_sem, self.recv_sem = send_sem, recv_sem
-        self.count = 0
-        self.started = []
+        self.groups, self.keys, self.steps = {}, {}, {}
         z, y, c, x = (lax.axis_index(a) for a in ("z", "y", "c", "x"))
         self.at = {"z": z, "y": y, "c": c, "x": x}
-        self.steps = {}
 
     def moved(self, **new):
         where = dict(self.at)
@@ -55,40 +54,32 @@
     def partner(self):
         return self.moved(c=1 - self.at["c"])
 
-    def send(self, src, dst, device):
-        k = self.count
-        self.count += 1
-        copy = pltpu.make_async_remote_copy(
+    def copy(self, src, dst, device, group, key):
+        return pltpu.make_async_remote_copy(
             src_ref=src,
             dst_ref=dst,
-            send_sem=self.send_sem.at[k],
-            recv_sem=self.recv_sem.at[k],
+            send_sem=self.send_sem.at[self.groups.setdefault(group, len(self.groups))],
+            recv_sem=self.recv_sem.at[self.keys.setdefault(key, len(self.keys))],
             device_id=device,
             device_id_type=MESH,
         )
-        copy.start()
-        self.started.append(copy)
-        return k
-
-    def arrived(self, k, dst):
-        pltpu.make_async_remote_copy(
-            src_ref=dst,
-            dst_ref=dst,
-            send_sem=self.send_sem.at[k],
-            recv_sem=self.recv_sem.at[k],
-            device_id=self.partner(),
-            device_id_type=MESH,
-        ).wait_recv()
-
-    def finish(self):
-        for copy in self.started:
-            copy.wait_send()
+
+    def send(self, src, dst, device, group, key):
+        self.copy(src, dst, device, group, key).start()
+
+    def arrived(self, key, size):
+        group = next(iter(self.groups))
+        self.copy(size, size, self.partner(), group, key).wait_recv()
+
+    def all_sent(self, group, size):
+        key = next(iter(self.keys))
+        self.copy(size, size, self.partner(), group, key).wait_send()
 
 
 class PlaneGather:
-    def __init__(self, wires, whole, depth, core):
-        self.w, self.whole, self.depth, self.core = wires, whole, depth, core
-        self.sent = {}
+    def __init__(self, wires, whole, width, depth, core, name):
+        self.w, self.whole, self.width = wires, whole, width
+        self.depth, self.core, self.name = depth, core, name
 
     def mixed(self, axis, one, two):
         first, second = (one, two) if axis == "z" else (two, one)
@@ -99,91 +90,104 @@
         start = ((z * RING + y) * 2 + self.core) * self.depth
         half = self.depth // 2
         if part is None:
-            return self.whole.at[pl.ds(pl.multiple_of(start, 16), self.depth)]
-        return self.whole.at[pl.ds(pl.multiple_of(start + part * half, 16), half)]
-
-    def go(self, name, d1, d2, first, distance, part=None):
+            return self.whole.at[pl.ds(pl.multiple_of(start, 16), self.depth), : self.width]
+        return self.whole.at[pl.ds(pl.multiple_of(start + part * half, 16), half), : self.width]
+
+    def go(self, key, d1, d2, first, distance, part=None):
         block = self.rows(d1, d2, part)
         one, two = (distance, 0) if first else (0, distance)
         device = self.w.moved(z=self.mixed("z", one, two), y=self.mixed("y", one, two))
-        self.sent[name] = self.w.send(block, block, device)
-
-    def came(self, name, d1, d2, part=None):
-        self.w.arrived(self.sent[name], self.rows(d1, d2, part))
+        self.w.send(block, block, device, self.name[0], key)
+
+    def came(self, key, blocks):
+        self.w.arrived(key, self.whole.at[pl.ds(0, blocks * self.depth), : self.width])
 
     def second_round(self, d1):
-        self.go(("b", 1, d1), d1, 0, False, 1)
-        self.go(("b", -1, d1), d1, 0, False, -1)
+        for side in (1, -1):
+            self.go((self.name, "second", d1), d1, 0, False, side)
 
     def start(self):
-        self.go(("a", 1), 0, 0, True, 1)
-        self.go(("a", -1), 0, 0, True, -1)
+        for side in (1, -1):
+            self.go((self.name, "first"), 0, 0, True, side)
         self.second_round(0)
 
-    def first_came(self, side):
-        self.came(("a", side), -side, 0)
-        self.go(("ah", side), -side, 0, True, side, 0 if side > 0 else 1)
-        self.second_round(-side)
-
-    def second_came(self, d1, side):
-        self.came(("b", side, d1), d1, -side)
-        self.go(("bh", side, d1), d1, -side, False, side, 0 if side > 0 else 1)
-
-    def first_done(self, side):
-        self.came(("ah", side), 2, 0, 0 if side > 0 else 1)
-        if side < 0:
-            self.second_round(2)
-
-    def second_done(self, d1, side):
-        self.came(("bh", side, d1), d1, 2, 0 if side > 0 else 1)
-
-
-def plane_steps(wires, whole, depth, own_ready, other_ready):
+    def first_came(self):
+        self.came((self.name, "first"), 2)
+        for side in (1, -1):
+            self.go((self.name, "again"), -side, 0, True, side, 0 if side > 0 else 1)
+            self.second_round(-side)
+
+    def second_came(self, d1):
+        self.came((self.name, "second", d1), 2)
+        for side in (1, -1):
+            self.go((self.name[0], "last"), d1, -side, False, side, 0 if side > 0 else 1)
+
+    def first_done(self):
+        self.came((self.name, "again"), 1)
+        self.second_round(2)
+
+    def all_done(self):
+        self.came((self.name[0], "last"), 8)
+
+    def all_sent(self):
+        self.w.all_sent(self.name[0], self.whole.at[pl.ds(0, 30 * self.depth), : self.width])
+
+
+def plane_steps(wires, whole, width, depth, name, own_ready, other_ready):
     c = wires.at["c"]
-    pair = [PlaneGather(wires, whole, depth, core) for core in (c, 1 - c)]
-    both = [(g, side) for side in (1, -1) for g in pair]
+    pair = [
+        PlaneGather(wires, whole, width, depth, core, (name, k))
+        for k, core in enumerate((c, 1 - c))
+    ]
     steps = [own_ready, pair[0].start, other_ready, pair[1].start]
-    steps += [functools.partial(g.first_came, side) for g, side in both]
-    steps += [functools.partial(g.second_came, 0, side) for g, side in both]
-    steps += [functools.partial(g.first_done, side) for g, side in both]
+    steps += [g.first_came for g in pair]
+    steps += [functools.partial(g.second_came, 0) for g in pair]
+    steps += [g.first_done for g in pair]
     for d1 in (-1, 1, 2):
-        steps += [functools.partial(g.second_came, d1, side) for g, side in both]
-    for d1 in (0, -1, 1, 2):
-        steps += [functools.partial(g.second_done, d1, side) for g, side in both]
-    return steps
+        steps += [functools.partial(g.second_came, d1) for g in pair]
+    return steps + [pair[0].all_done], pair[0].all_sent
 
 
 class RowGather:
-    def __init__(self, wires, region):
-        self.w, self.region = wires, region
+    def __init__(self, wires, region, group, name, relative=False):
+        self.w, self.region, self.relative = wires, region, relative
+        self.group, self.name = group, name
 
     def piece(self, dx, other=False, part=None):
         c = self.w.at["c"]
-        return self.region(self.w.step("x", dx), 1 - c if other else c, part)
+        where = dx if self.relative else self.w.step("x", dx)
+        return self.region(where, 1 - c if other else c, part)
+
+    def there(self, dx, side, part=None):
+        if self.relative:
+            dx = (0, 1, 2, -1)[(dx - side) % RING]
+        return self.piece(dx, part=part)
+
+    def share(self, dx):
+        block = self.piece(dx)
+        key = (self.group, "shared", self.relative and dx in (1, 2))
+        self.w.send(block, block, self.w.partner(), self.group, key)
 
     def start(self):
-        own, w = self.piece(0), self.w
-        self.right = w.send(own, own, w.neighbour("x", 1))
-        self.left = w.send(own, own, w.neighbour("x", -1))
-        self.over = {0: w.send(own, own, w.partner())}
-        self.again = {}
+        for side in (1, -1):
+            self.w.send(
+                self.piece(0), self.there(0, side), self.w.neighbour("x", side),
+                self.group, (self.group, self.name, side),
+            )
+        self.share(0)
 
     def came(self, side):
-        w, part = self.w, 0 if side > 0 else 1
-        block, half = self.piece(-side), self.piece(-side, part=part)
-        w.arrived(self.right if side > 0 else self.left, block)
-        self.again[side] = w.send(half, half, w.neighbour("x", side))
-        self.over[-side] = w.send(block, block, w.partner())
-
-    def done(self, side):
-        w = self.w
-        w.arrived(self.again[side], self.piece(2, part=0 if side > 0 else 1))
-        if side < 0:
-            block = self.piece(2)
-            self.over[2] = w.send(block, block, w.partner())
-
-    def shared(self, dx):
-        self.w.arrived(self.over[dx], self.piece(dx, other=True))
+        part = 0 if side > 0 else 1
+        self.w.arrived((self.group, self.name, side), self.piece(-side))
+        self.w.send(
+            self.piece(-side, part=part), self.there(-side, side, part),
+            self.w.neighbour("x", side), self.group, (self.group, self.name, 0),
+        )
+        self.share(-side)
+
+    def done(self):
+        self.w.arrived((self.group, self.name, 0), self.piece(2))
+        self.share(2)
 
 
 def dot(a, b, dims=((1,), (0,))):
@@ -225,7 +229,7 @@
     tok, gain, wq, wk, wv, wmq, wmk, wmv, wmg, wo, wg, sinks, fbias, fshift,
     out, lt_out,
     tokv, rawkv, kvp, normed, w1, w2, w3, wgv, p1, gate, p2, kd, vd, sh, msgs, pre, outs, lt, ltin,
-    stage, total, turned, small, rows_in, rows_f, rows_sh, square, send_sem, recv_sem, local_sem,
+    stage, turned, small, rows_in, rows_f, rows_sh, square, send_sem, recv_sem, local_sem,
 ):
     bf, f32 = jnp.bfloat16, jnp.float32
     w = Wires(send_sem, recv_sem)
@@ -279,19 +283,21 @@
     kept[1] = fetch(kvp.at[c], block_rows(w1, c, 128, slice(256, 384)))
     pl.semaphore_wait(barrier, len(greeted))
 
-    over = [
-        w.send(half_of(1 - c), block_rows(dst, c, depth, cols), w.partner())
-        for half_of, dst, depth, cols in pieces
-    ]
-
-    def token_rows(xi, ci, part):
-        start = (ci * RING + xi) * TOK
+    sizes = (w1.at[0:128, 0:640], w2.at[0:128, :], w3.at[0:96, :])
+    for n, (half_of, dst, depth, cols) in enumerate(pieces):
+        key = ("over", (n >= 4) + (n >= 6))
+        w.send(half_of(1 - c), block_rows(dst, c, depth, cols), w.partner(), "over", key)
+
+    slots = {0: 0, -1: 1, 1: 2, 2: 3}
+
+    def token_rows(dx, ci, part):
+        start = slots[dx] * 2 * TOK + ci * TOK
         if part is None:
             return normed.at[pl.ds(pl.multiple_of(start, 16), TOK)]
         return normed.at[pl.ds(pl.multiple_of(start + part * (TOK // 2), 16), TOK // 2)]
 
-    tokens = RowGather(w, token_rows)
-    first_row = (c * RING + x) * TOK
+    tokens = RowGather(w, token_rows, "tokens", "", relative=True)
+    first_row = c * TOK
 
     def normalize(i, carry):
         values = tokv[pl.ds(pl.multiple_of(i * 16, 16), 16), :].astype(f32)
@@ -301,24 +307,25 @@
         ).astype(bf)
         return carry
 
-    shift_over = w.send(fshift, sh.at[c], w.partner())
+    w.send(fshift, sh.at[c], w.partner(), "shift", "shift")
 
     def own_ready(first, last):
         for n in range(first, last):
             kept[n].wait()
 
-    def other_ready(first, last):
-        for n in range(first, last):
-            _, dst, depth, cols = pieces[n]
-            w.arrived(over[n], block_rows(dst, 1 - c, depth, cols))
-
-    groups = [
-        plane_steps(
-            w, whole, depth,
-            functools.partial(own_ready, *span), functools.partial(other_ready, *span),
+    def other_ready(group):
+        w.arrived(("over", group), sizes[group])
+
+    groups, sent = [], []
+    for n, (whole, width, depth, pair) in enumerate(
+        ((w1, 640, 128, (0, 4)), (w2, 256, 128, (4, 6)), (w3, 512, 96, (6, 7)))
+    ):
+        steps, all_sent = plane_steps(
+            w, whole, width, depth, ("weights", n),
+            functools.partial(own_ready, *pair), functools.partial(other_ready, n),
         )
-        for whole, depth, span in ((w1, 128, (0, 4)), (w2, 128, (4, 6)), (w3, 96, (6, 7)))
-    ]
+        groups.append(steps)
+        sent.append(all_sent)
     at = [0, 0, 0]
 
     def pump(group, upto):
@@ -326,22 +333,42 @@
             groups[group][at[group]]()
             at[group] += 1
 
-    def first_projection(i):
-        rows = slice(i * HALF, (i + 1) * HALF)
-        both = dot(normed[rows, :], w1[...])
-        p2[rows, :] = both[:, :256].astype(bf)
-        kv = both[:, 256:384]
+    def pieces_of(i):
+        for j in range(4):
+            dx, ci = (0, -1, 1, 2)[2 * i + j // 2], j % 2
+            yield slice(j * TOK, (j + 1) * TOK), (ci * RING + w.step("x", dx)) * TOK
+
+    def span(start):
+        return pl.ds(pl.multiple_of(start, 16), TOK)
+
+    def gate_weights():
+        gate_copy.wait()
+        for k in range(D // 128):
+            turned_gates = jnp.transpose(wgv[:, k * 128 : (k + 1) * 128].astype(f32))
+            w1[k * 128 : (k + 1) * 128, 640:672] = turned_gates.astype(bf)
+
+    def attn_projection(i):
+        both = dot(normed[i * HALF : (i + 1) * HALF, :], w1[:, :384])
+        kv = both[:, 256:]
         turned_kv = pltpu.roll(kv, HD, 1)
         lane = lax.broadcasted_iota(jnp.int32, kv.shape, 1)
-        after = slice(i * HALF + WINDOW, (i + 1) * HALF + WINDOW)
-        kd[after, :] = by_head(lane, kv, turned_kv).astype(bf)
-        vd[after, :] = by_head(lane, turned_kv, kv).astype(bf)
-        p1[rows, 0:256] = both[:, 384:].astype(bf)
-        gate[rows, 0:32] = dot(normed[rows, :], wgv[...], ((1,), (1,)))
+        keys = by_head(lane, kv, turned_kv).astype(bf)
+        values = by_head(lane, turned_kv, kv).astype(bf)
+        for rows, start in pieces_of(i):
+            p2[span(start), :] = both[rows, :256].astype(bf)
+            kd[span(start + WINDOW), :] = keys[rows]
+            vd[span(start + WINDOW), :] = values[rows]
+
+    def first_projection(i):
+        both = dot(normed[i * HALF : (i + 1) * HALF, :], w1[:, 384:])
+        for rows, start in pieces_of(i):
+            p1[span(start), 0:256] = both[rows, :256].astype(bf)
+            gate[span(start), 0:32] = both[rows, 256:]
 
     def second_projection(i):
-        rows = slice(i * HALF, (i + 1) * HALF)
-        p1[rows, 256:512] = dot(normed[rows, :], w2[...]).astype(bf)
+        both = dot(normed[i * HALF : (i + 1) * HALF, :], w2[...]).astype(bf)
+        for rows, start in pieces_of(i):
+            p1[span(start), 256:512] = both[rows]
 
     lane1 = lax.broadcasted_iota(jnp.int32, (1, 128), 1)
     lane = lax.broadcasted_iota(jnp.int32, (128, 128), 1)
@@ -356,7 +383,7 @@
         rows_sh[...] = jnp.zeros_like(rows_sh)
         gate[:, 32:] = jnp.zeros((ROWS, 96), f32)
         square[...] = jnp.zeros_like(square)
-        w.arrived(shift_over, sh.at[1 - c])
+        w.arrived("shift", sh.at[1 - c])
         for b in range(BLOCKS):
             turned[...] = jnp.transpose(gate[b * BLK : (b + 1) * BLK, :])
             for h in range(2):
@@ -416,17 +443,14 @@
         msgs[chip, 0:HD, :] = state[1].astype(bf)
         msgs[chip, HD : HD + 16, :] = small[...].astype(bf)
 
-    told = []
-
     def tell_state():
         mine = msgs.at[chip]
         for dz, dy in plane:
             device = w.moved(z=w.step("z", dz), y=w.step("y", dy))
-            told.append(w.send(mine, mine, device))
+            w.send(mine, mine, device, "state", "state")
 
     def incoming_state():
-        for k, (dz, dy) in zip(told, plane):
-            w.arrived(k, msgs.at[w.step("z", -dz) * RING + w.step("y", -dy)])
+        w.arrived("state", msgs.at[0 : CHIPS - 1])
         state = (
             jnp.zeros((1, 128), f32), jnp.zeros((HD, 128), f32), jnp.zeros((1, 128), f32),
             jnp.full((1, 128), MASKED, f32),
@@ -506,17 +530,17 @@
 
     third = ROWS // 3
 
-    def out_region(start, base, stride, width):
+    def out_region(start, base, stride, width, group):
         def region(xi, ci, part):
             count = third if part is None else third // 2
             first = start if part is None else start + part * (third // 2)
             col = pl.multiple_of(base + 2 * stride * xi + stride * ci, 128)
             return outs.at[pl.ds(first, count), pl.ds(col, width)]
 
-        return RowGather(w, region)
-
-    mem_out = [out_region(i * third, 2048, 128, 128) for i in range(3)]
-    attn_out = [out_region(i * third, 0, 256, 256) for i in range(3)]
+        return RowGather(w, region, group, start)
+
+    mem_out = [out_region(i * third, 2048, 128, 128, "mem") for i in range(3)]
+    attn_out = [out_region(i * third, 0, 256, 256, "attn") for i in range(3)]
     theirs = pl.ds(pl.multiple_of((1 - c) * HALF, HALF), HALF)
     ours = pl.ds(pl.multiple_of(c * HALF, HALF), HALF)
 
@@ -528,13 +552,30 @@
 
     def rim_start():
         next_chip = w.moved(z=lax.rem(z + (y + 1) // RING, RING), y=w.step("y", 1))
-        kept_values["rim"] = [
-            w.send(ref.at[ROWS : ROWS + WINDOW], ref.at[0:WINDOW], next_chip) for ref in (kd, vd)
-        ]
+        for ref in (kd, vd):
+            w.send(ref.at[ROWS : ROWS + WINDOW], ref.at[0:WINDOW], next_chip, "rim", "rim")
 
     def rim_came():
-        w.arrived(kept_values["rim"][0], kd.at[0:WINDOW])
-        w.arrived(kept_values["rim"][1], vd.at[0:WINDOW])
+        w.arrived("rim", kd.at[0 : 2 * WINDOW])
+
+    def tokens_shared(late):
+        w.arrived(("tokens", "shared", bool(late)), normed.at[0 : 2 * TOK])
+
+    def attn_shared():
+        w.arrived(("attn", "shared", False), outs.at[:, 0:1024])
+
+    def mem_shared():
+        w.arrived(("mem", "shared", False), outs.at[:, 0:512])
+
+    def finish():
+        for all_sent in sent:
+            all_sent()
+        for group, size in (
+            ("over", w1.at[0:256, 0:640]), ("tokens", normed.at[0 : 7 * TOK]), ("shift", sh.at[0]),
+            ("state", msgs.at[0 : CHIPS - 1]), ("rim", kd.at[0 : 2 * WINDOW]),
+            ("attn", outs.at[:, 0:1792]), ("mem", outs.at[:, 0:896]), ("log", ltin), ("out", stage),
+        ):
+            w.all_sent(group, size)
 
     def state_came():
         kept_values["state"] = incoming_state()
@@ -543,32 +584,28 @@
         for b in range(first, last):
             memory_block(b, kept_values["state"])
 
-    def out_first(half):
-        rows = (theirs, ours)[half]
-        total[rows, :] = dot(outs[rows, :2048], w3[:2048])
-
     def log_start():
-        kept_values["log"] = w.send(lt.at[theirs], ltin, w.partner())
+        w.send(lt.at[theirs], ltin, w.partner(), "log", "log")
 
     def out_last():
         out_cols = out.at[:, pl.ds(pl.multiple_of(c * 512, 512), 512)]
-        stage[...] = (total[theirs, :] + dot(outs[theirs, 2048:], w3[2048:])).astype(bf)
-        mixed_over = w.send(stage, out_cols, w.partner())
-        out[:, pl.ds(pl.multiple_of(c * 512, 512), 512)] = (
-            total[ours, :] + dot(outs[ours, 2048:], w3[2048:])
+        stage[...] = dot(outs[theirs, :], w3[...]).astype(bf)
+        w.send(stage, out_cols, w.partner(), "out", "out")
+        out[:, pl.ds(pl.multiple_of(c * 512, 512), 512)] = dot(
+            outs[ours, :], w3[...]
         ).astype(bf)
-        w.arrived(kept_values["log"], ltin)
+        w.arrived("log", ltin)
         lt_out[...] = jnp.transpose(lt[ours, :] + ltin[...])[:8]
-        w.arrived(mixed_over, out.at[:, pl.ds(pl.multiple_of((1 - c) * 512, 512), 512)])
+        w.arrived("out", out.at[:, pl.ds(pl.multiple_of((1 - c) * 512, 512), 512)])
 
     schedule(
         types.SimpleNamespace(
-            pump=pump, normalize=normalize_all, finish=w.finish, tokens=tokens, gate_weights=gate_copy.wait,
-            first_projection=first_projection, second_projection=second_projection,
+            pump=pump, normalize=normalize_all, finish=finish, tokens_shared=tokens_shared,
+            attn_shared=attn_shared, mem_shared=mem_shared, tokens=tokens, gate_weights=gate_weights,
+            attn_projection=attn_projection, first_projection=first_projection, second_projection=second_projection,
             rim_start=rim_start, rim_came=rim_came, memory_gates=memory_gates,
             tell_state=tell_state, state_came=state_came, memory_blocks=memory_blocks,
-            attention=attention, attn_out=attn_out, mem_out=mem_out, out_first=out_first,
-            log_start=log_start, out_last=out_last,
+            attention=attention, attn_out=attn_out, mem_out=mem_out, log_start=log_start, out_last=out_last,
         )
     )
 
@@ -578,113 +615,76 @@
     pump(0, 2)
     s.normalize()
     s.tokens.start()
-    pump(0, 21)
-    pump(1, 4)
-    pump(0, 23)
+    pump(0, 8)
+    s.gate_weights()
+    pump(0, 14)
     s.tokens.came(1)
     s.tokens.came(-1)
-    pump(0, 35)
+    s.tokens_shared(0)
+    pump(0, 16)
+    pump(1, 4)
+    pump(0, 17)
+    s.attn_projection(0)
     pump(1, 5)
-    pump(0, 37)
-    pump(1, 11)
-    pump(0, 39)
-    pump(1, 12)
-    s.tokens.done(1)
-    s.tokens.done(-1)
-    s.tokens.shared(0)
-    s.tokens.shared(-1)
-    s.tokens.shared(1)
-    pump(0, 43)
+    s.tokens.done()
+    s.first_projection(0)
+    pump(1, 8)
+    s.tokens_shared(1)
+    s.attn_projection(1)
+    pump(1, 9)
+    s.rim_start()
+    s.attention(2, 4)
+    attn[1].start()
     pump(1, 13)
-    s.tokens.shared(2)
-    pump(0, 44)
-    s.gate_weights()
-    s.first_projection(0)
-    pump(1, 24)
+    s.attention(4, 6)
+    attn[2].start()
+    pump(1, 15)
     pump(2, 4)
     s.first_projection(1)
-    pump(1, 32)
-    s.rim_start()
-    s.memory_gates()
-    pump(1, 40)
-    s.tell_state()
-    s.attention(2, 4)
-    attn[1].start()
-    s.attention(4, 6)
-    attn[2].start()
-    pump(2, 12)
-    pump(1, 44)
-    s.second_projection(0)
+    pump(1, 16)
     s.rim_came()
     s.attention(0, 2)
     attn[0].start()
     attn[1].came(1)
     attn[1].came(-1)
-    s.second_projection(1)
+    s.log_start()
+    s.memory_gates()
+    s.tell_state()
+    pump(2, 5)
     attn[2].came(1)
     attn[2].came(-1)
-    s.log_start()
-    pump(2, 13)
+    pump(2, 8)
+    pump(1, 17)
+    s.second_projection(0)
+    attn[0].came(1)
+    attn[0].came(-1)
+    s.second_projection(1)
+    attn[1].done()
+    attn[2].done()
+    attn[0].done()
+    pump(2, 9)
     s.state_came()
     s.memory_blocks(0, 2)
     mem[0].start()
-    attn[0].came(1)
-    attn[0].came(-1)
+    s.attn_shared()
     s.memory_blocks(2, 4)
     mem[1].start()
-    pump(2, 15)
-    attn[1].done(1)
-    attn[1].done(-1)
-    attn[1].shared(0)
-    attn[1].shared(-1)
-    attn[1].shared(1)
     s.memory_blocks(4, 6)
     mem[2].start()
-    pump(2, 24)
-    attn[1].shared(2)
-    attn[2].done(1)
-    attn[2].done(-1)
-    attn[2].shared(0)
-    attn[2].shared(-1)
-    attn[2].shared(1)
+    pump(2, 14)
     mem[0].came(1)
     mem[0].came(-1)
-    attn[2].shared(2)
-    attn[0].done(1)
-    attn[0].done(-1)
-    attn[0].shared(0)
-    attn[0].shared(-1)
-    attn[0].shared(1)
-    pump(2, 25)
-    attn[0].shared(2)
     mem[1].came(1)
     mem[1].came(-1)
-    pump(2, 33)
+    pump(2, 15)
     mem[2].came(1)
     mem[2].came(-1)
-    pump(2, 37)
-    mem[0].done(1)
-    mem[0].done(-1)
-    mem[0].shared(0)
-    mem[0].shared(-1)
-    mem[0].shared(1)
-    pump(2, 41)
-    mem[1].done(1)
-    mem[1].done(-1)
-    mem[1].shared(0)
-    mem[1].shared(-1)
-    mem[1].shared(1)
-    mem[0].shared(2)
-    pump(2, 44)
-    s.out_first(0)
-    mem[1].shared(2)
-    mem[2].done(1)
-    mem[2].done(-1)
-    mem[2].shared(0)
-    mem[2].shared(-1)
-    mem[2].shared(1)
-    s.out_first(1)
-    mem[2].shared(2)
+    pump(2, 16)
+    mem[0].done()
+    mem[1].done()
+    mem[2].done()
+    s.mem_shared()
+    pump(2, 17)
     s.out_last()
     s.finish()
 
@@ -701,8 +701,8 @@
     mixed, log_total = pl.pallas_call(
         layer_kernel,
         out_shape=[
-            jax.ShapeDtypeStruct((HALF, 1024), bf),
-            jax.ShapeDtypeStruct((8, HALF), f32),
+            pltpu.VMEM((HALF, 1024), bf),
+            pltpu.VMEM((8, HALF), f32),
         ],
         in_specs=[anywhere, vmem] + [anywhere] * 9 + [smem, smem, vmem],
         out_specs=[vmem, vmem],
@@ -711,7 +711,7 @@
             pltpu.VMEM((2, 128, 128), bf),
             pltpu.VMEM((2, 128, 128), bf),
             pltpu.VMEM((ROWS, D), bf),
-            pltpu.VMEM((D, 640), bf),
+            pltpu.VMEM((D, 672), bf),
             pltpu.VMEM((D, 256), bf),
             pltpu.VMEM((3072, 512), bf),
             pltpu.VMEM((32, D), bf),
@@ -727,16 +727,15 @@
             pltpu.VMEM((ROWS, 128), f32),
             pltpu.VMEM((HALF, 128), f32),
             pltpu.VMEM((HALF, 512), bf),
-            pltpu.VMEM((ROWS, 512), f32),
             pltpu.VMEM((128, 128), f32),
             pltpu.VMEM((16, 128), f32),
             pltpu.VMEM((16, 128), f32),
             pltpu.VMEM((16, 128), f32),
             pltpu.VMEM((16, 128), f32),
             pltpu.VMEM((128, 128), f32),
-            pltpu.SemaphoreType.DMA((MAX_COPIES,)),
-            pltpu.SemaphoreType.DMA((MAX_COPIES,)),
-            pltpu.SemaphoreType.DMA((16,)),
+            pltpu.SemaphoreType.DMA((SENDS,)),
+            pltpu.SemaphoreType.DMA((RECEIVES,)),
+            pltpu.SemaphoreType.DMA((11,)),
         ],
         compiler_params=pltpu.CompilerParams(
             collective_id=0, has_side_effects=True, vmem_limit_bytes=60 * 1024 * 1024

time: 91 us -> 83.6 us (0.919)
  Pallas kernels: 86.3 us -> 80 us
  local copies, waits for them, and re-layouts: 2.67 us -> 1.48 us
    pallas_call x1, Pallas kernels: 86.3 us -> 80 us  [shards(): pl.pallas_call(layer_kernel, out_shape=[pltpu.VMEM((HALF, 1024), bf), plt...]
    unnamed x4 -> x2, local copies, waits for them, and re-layouts: 2.67 us -> 1.48 us
where the time goes in v4:
time: 83.6 us; the launch traced here: 82.1 us
  Pallas kernels  80 us (96%)
  local copies, waits for them, and re-layouts  1.48 us (2%)
    pallas_call x1, Pallas kernels, shards(): pl.pallas_call(layer_kernel, out_shape=[pltpu.VMEM((HALF, 1024), bf), plt...  80 us

profile of v4, /device:TPU:0, one launch (start us, length us, event | category | flops | bytes accessed | tf_op | source)
XLA Modules:
  0.0 82.1 jit_solution(4452819801019994487)
XLA Ops:
  0.6 80.0 %layer.1 = (bf16[384,1024]{1,0:T(8,128)(2,1)S(1)}, f32[8,384]{1,0:T(8,128)S(1)}) custom-call(bf16[96,4096]{1,0:T(8,128)(2,1)} %tok.1, f32[1,4096]{1,0:T(1,128)} %bitcast.8, bf16[128,512]{1,0:T(8,128)(2,1)} %wq.1, bf16[128,128]{1,0:T(8,128)(2,1)} %wk.1, bf16[128,128]{1,0:T(8,128)(2,1)} %wv.1, bf16[128,256]{1,0:T(8,128)(2,1)} %wmq.1, bf16[128,256]{1,0:T(8,128)(2,1)} %wmk.1, ...), custom_call_target="tpu_custom_call" | custom-call | tf_op jit(solution)/shard_map/layer/pallas_call | solution.py:701
  80.6 0.9 %copy.18 = bf16[384,1024]{1,0:T(8,128)(2,1)} copy(bf16[384,1024]{1,0:T(8,128)(2,1)S(1)} %get-tuple-element.6) | data formatting | bytes 1572864
  81.5 0.6 copy.19

commit v5 on v4

--- a/solution.py
+++ b/solution.py
@@ -21,8 +21,8 @@
 ROWS = 8 * TOK
 D = 4096
 PLANE = ("z", "y")
-SENDS = 12
-RECEIVES = 72
+SENDS = 26
+RECEIVES = 86
 HALF = ROWS // 2
 BLOCKS = ROWS // BLK
 CHIPS = RING * RING
@@ -34,6 +34,9 @@
         self.groups, self.keys, self.steps = {}, {}, {}
         z, y, c, x = (lax.axis_index(a) for a in ("z", "y", "c", "x"))
         self.at = {"z": z, "y": y, "c": c, "x": x}
+        for axis in ("z", "y", "x"):
+            for distance in range(1, RING):
+                self.step(axis, distance)
 
     def moved(self, **new):
         where = dict(self.at)
@@ -63,6 +66,10 @@
             device_id=device,
             device_id_type=MESH,
         )
+
+    def reserve(self, group, key):
+        self.groups.setdefault(group, len(self.groups))
+        self.keys.setdefault(key, len(self.keys))
 
     def send(self, src, dst, device, group, key):
         self.copy(src, dst, device, group, key).start()
@@ -229,7 +236,7 @@
     tok, gain, wq, wk, wv, wmq, wmk, wmv, wmg, wo, wg, sinks, fbias, fshift,
     out, lt_out,
     tokv, rawkv, kvp, normed, w1, w2, w3, wgv, p1, gate, p2, kd, vd, sh, msgs, pre, outs, lt, ltin,
-    stage, turned, small, rows_in, rows_f, rows_sh, square, send_sem, recv_sem, local_sem,
+    stage, total, turned, small, rows_in, rows_f, rows_sh, square, send_sem, recv_sem, local_sem,
 ):
     bf, f32 = jnp.bfloat16, jnp.float32
     w = Wires(send_sem, recv_sem)
@@ -443,14 +450,27 @@
         msgs[chip, 0:HD, :] = state[1].astype(bf)
         msgs[chip, HD : HD + 16, :] = small[...].astype(bf)
 
+    def chip_at(dz, dy):
+        return w.step("z", dz) * RING + w.step("y", dy)
+
     def tell_state():
         mine = msgs.at[chip]
         for dz, dy in plane:
-            device = w.moved(z=w.step("z", dz), y=w.step("y", dy))
-            w.send(mine, mine, device, "state", "state")
+            key = ("state", dz, dy)
+            w.reserve(key, key)
+
+            @pl.when(chip_at(dz, dy) > chip)
+            def _():
+                device = w.moved(z=w.step("z", dz), y=w.step("y", dy))
+                w.send(mine, mine, device, key, key)
 
     def incoming_state():
-        w.arrived("state", msgs.at[0 : CHIPS - 1])
+        for dz, dy in plane:
+
+            @pl.when(chip_at(-dz, -dy) < chip)
+            def _():
+                w.arrived(("state", dz, dy), msgs.at[0])
+
         state = (
             jnp.zeros((1, 128), f32), jnp.zeros((HD, 128), f32), jnp.zeros((1, 128), f32),
             jnp.full((1, 128), MASKED, f32),
@@ -572,10 +592,15 @@
             all_sent()
         for group, size in (
             ("over", w1.at[0:256, 0:640]), ("tokens", normed.at[0 : 7 * TOK]), ("shift", sh.at[0]),
-            ("state", msgs.at[0 : CHIPS - 1]), ("rim", kd.at[0 : 2 * WINDOW]),
+            ("rim", kd.at[0 : 2 * WINDOW]),
             ("attn", outs.at[:, 0:1792]), ("mem", outs.at[:, 0:896]), ("log", ltin), ("out", stage),
         ):
             w.all_sent(group, size)
+        for dz, dy in plane:
+
+            @pl.when(chip_at(dz, dy) > chip)
+            def _():
+                w.all_sent(("state", dz, dy), msgs.at[0])
 
     def state_came():
         kept_values["state"] = incoming_state()
@@ -584,15 +609,19 @@
         for b in range(first, last):
             memory_block(b, kept_values["state"])
 
+    def out_first(half):
+        rows = (theirs, ours)[half]
+        total[rows, :] = dot(outs[rows, :2048], w3[:2048])
+
     def log_start():
         w.send(lt.at[theirs], ltin, w.partner(), "log", "log")
 
     def out_last():
         out_cols = out.at[:, pl.ds(pl.multiple_of(c * 512, 512), 512)]
-        stage[...] = dot(outs[theirs, :], w3[...]).astype(bf)
+        stage[...] = (total[theirs, :] + dot(outs[theirs, 2048:], w3[2048:])).astype(bf)
         w.send(stage, out_cols, w.partner(), "out", "out")
-        out[:, pl.ds(pl.multiple_of(c * 512, 512), 512)] = dot(
-            outs[ours, :], w3[...]
+        out[:, pl.ds(pl.multiple_of(c * 512, 512), 512)] = (
+            total[ours, :] + dot(outs[ours, 2048:], w3[2048:])
         ).astype(bf)
         w.arrived("log", ltin)
         lt_out[...] = jnp.transpose(lt[ours, :] + ltin[...])[:8]
@@ -605,7 +634,7 @@
             attn_projection=attn_projection, first_projection=first_projection, second_projection=second_projection,
             rim_start=rim_start, rim_came=rim_came, memory_gates=memory_gates,
             tell_state=tell_state, state_came=state_came, memory_blocks=memory_blocks,
-            attention=attention, attn_out=attn_out, mem_out=mem_out, log_start=log_start, out_last=out_last,
+            attention=attention, attn_out=attn_out, mem_out=mem_out, log_start=log_start, out_first=out_first, out_last=out_last,
         )
     )
 
@@ -633,58 +662,68 @@
     s.attn_projection(1)
     pump(1, 9)
     s.rim_start()
-    s.attention(2, 4)
-    attn[1].start()
+    s.attention(3, 4)
+    s.attention(5, 6)
     pump(1, 13)
-    s.attention(4, 6)
-    attn[2].start()
+    s.first_projection(1)
+    pump(1, 14)
+    pump(2, 2)
     pump(1, 15)
     pump(2, 4)
-    s.first_projection(1)
+    s.attention(4, 5)
+    attn[2].start()
+    s.memory_gates()
     pump(1, 16)
     s.rim_came()
-    s.attention(0, 2)
+    s.attention(0, 1)
+    s.tell_state()
+    s.attention(2, 3)
+    attn[1].start()
+    s.attention(1, 2)
     attn[0].start()
-    attn[1].came(1)
-    attn[1].came(-1)
+    pump(2, 5)
     s.log_start()
-    s.memory_gates()
-    s.tell_state()
-    pump(2, 5)
     attn[2].came(1)
     attn[2].came(-1)
     pump(2, 8)
     pump(1, 17)
     s.second_projection(0)
+    attn[1].came(1)
+    attn[1].came(-1)
+    s.second_projection(1)
+    pump(2, 9)
+    s.state_came()
     attn[0].came(1)
     attn[0].came(-1)
-    s.second_projection(1)
+    s.memory_blocks(0, 1)
+    s.memory_blocks(1, 2)
+    mem[0].start()
+    attn[2].done()
+    s.memory_blocks(2, 3)
+    s.memory_blocks(3, 4)
+    mem[1].start()
     attn[1].done()
-    attn[2].done()
+    s.memory_blocks(4, 5)
+    pump(2, 14)
+    s.memory_blocks(5, 6)
+    mem[2].start()
     attn[0].done()
-    pump(2, 9)
-    s.state_came()
-    s.memory_blocks(0, 2)
-    mem[0].start()
-    s.attn_shared()
-    s.memory_blocks(2, 4)
-    mem[1].start()
-    s.memory_blocks(4, 6)
-    mem[2].start()
-    pump(2, 14)
     mem[0].came(1)
     mem[0].came(-1)
+    s.attn_shared()
+    pump(2, 15)
     mem[1].came(1)
     mem[1].came(-1)
-    pump(2, 15)
+    pump(2, 16)
     mem[2].came(1)
     mem[2].came(-1)
-    pump(2, 16)
     mem[0].done()
     mem[1].done()
+    pump(2, 17)
+    s.out_first(0)
     mem[2].done()
+    s.out_first(1)
     s.mem_shared()
-    pump(2, 17)
     s.out_last()
     s.finish()
 
@@ -727,6 +766,7 @@
             pltpu.VMEM((ROWS, 128), f32),
             pltpu.VMEM((HALF, 128), f32),
             pltpu.VMEM((HALF, 512), bf),
+            pltpu.VMEM((ROWS, 512), f32),
             pltpu.VMEM((128, 128), f32),
             pltpu.VMEM((16, 128), f32),
             pltpu.VMEM((16, 128), f32),

time: 83.6 us -> 82 us (0.981)
  Pallas kernels: 80 us -> 78.5 us
    pallas_call x1, Pallas kernels: 80 us -> 78.5 us  [shards(): pl.pallas_call(layer_kernel, out_shape=[pltpu.VMEM((HALF, 1024), bf), plt...]
where the time goes in v5:
time: 82 us; the launch traced here: 80.7 us
  Pallas kernels  78.5 us (96%)
  local copies, waits for them, and re-layouts  1.48 us (2%)
    pallas_call x1, Pallas kernels, shards(): pl.pallas_call(layer_kernel, out_shape=[pltpu.VMEM((HALF, 1024), bf), plt...  78.5 us

profile of v5, /device:TPU:0, one launch (start us, length us, event | category | flops | bytes accessed | tf_op | source)
XLA Modules:
  0.0 80.7 jit_solution(2987581421155624420)
XLA Ops:
  0.6 78.5 %layer.1 = (bf16[384,1024]{1,0:T(8,128)(2,1)S(1)}, f32[8,384]{1,0:T(8,128)S(1)}) custom-call(bf16[96,4096]{1,0:T(8,128)(2,1)} %tok.1, f32[1,4096]{1,0:T(1,128)} %bitcast.8, bf16[128,512]{1,0:T(8,128)(2,1)} %wq.1, bf16[128,128]{1,0:T(8,128)(2,1)} %wk.1, bf16[128,128]{1,0:T(8,128)(2,1)} %wv.1, bf16[128,256]{1,0:T(8,128)(2,1)} %wmq.1, bf16[128,256]{1,0:T(8,128)(2,1)} %wmk.1, ...), custom_call_target="tpu_custom_call" | custom-call | tf_op jit(solution)/shard_map/layer/pallas_call | solution.py:740
  79.2 0.9 %copy.18 = bf16[384,1024]{1,0:T(8,128)(2,1)} copy(bf16[384,1024]{1,0:T(8,128)(2,1)S(1)} %get-tuple-element.6) | data formatting | bytes 1572864
  80.1 0.6 copy.19

commit v6 on v5

--- a/solution.py
+++ b/solution.py
@@ -647,81 +647,80 @@
     pump(0, 8)
     s.gate_weights()
     pump(0, 14)
+    pump(1, 4)
     s.tokens.came(1)
     s.tokens.came(-1)
+    pump(0, 16)
+    s.tokens.done()
+    pump(1, 6)
+    pump(1, 8)
+    pump(0, 17)
     s.tokens_shared(0)
-    pump(0, 16)
-    pump(1, 4)
-    pump(0, 17)
+    s.first_projection(0)
+    pump(1, 9)
     s.attn_projection(0)
-    pump(1, 5)
-    s.tokens.done()
-    s.first_projection(0)
-    pump(1, 8)
+    pump(1, 14)
+    pump(2, 4)
     s.tokens_shared(1)
     s.attn_projection(1)
-    pump(1, 9)
     s.rim_start()
+    s.attention(4, 5)
+    pump(1, 15)
+    s.attention(2, 3)
     s.attention(3, 4)
+    attn[1].start()
+    s.first_projection(1)
+    pump(1, 16)
+    s.memory_gates()
+    s.tell_state()
+    s.attention(1, 2)
+    pump(2, 5)
     s.attention(5, 6)
-    pump(1, 13)
-    s.first_projection(1)
-    pump(1, 14)
-    pump(2, 2)
-    pump(1, 15)
-    pump(2, 4)
-    s.attention(4, 5)
     attn[2].start()
-    s.memory_gates()
-    pump(1, 16)
+    pump(2, 7)
+    attn[1].came(1)
+    attn[1].came(-1)
+    pump(2, 8)
     s.rim_came()
     s.attention(0, 1)
-    s.tell_state()
-    s.attention(2, 3)
-    attn[1].start()
-    s.attention(1, 2)
     attn[0].start()
-    pump(2, 5)
+    pump(1, 17)
+    s.second_projection(0)
+    s.second_projection(1)
     s.log_start()
+    pump(2, 9)
     attn[2].came(1)
     attn[2].came(-1)
-    pump(2, 8)
-    pump(1, 17)
-    s.second_projection(0)
-    attn[1].came(1)
-    attn[1].came(-1)
-    s.second_projection(1)
-    pump(2, 9)
     s.state_came()
-    attn[0].came(1)
-    attn[0].came(-1)
     s.memory_blocks(0, 1)
     s.memory_blocks(1, 2)
     mem[0].start()
-    attn[2].done()
+    attn[1].done()
     s.memory_blocks(2, 3)
     s.memory_blocks(3, 4)
     mem[1].start()
-    attn[1].done()
     s.memory_blocks(4, 5)
-    pump(2, 14)
     s.memory_blocks(5, 6)
     mem[2].start()
-    attn[0].done()
+    pump(2, 14)
+    attn[0].came(1)
+    attn[0].came(-1)
+    attn[2].done()
     mem[0].came(1)
     mem[0].came(-1)
-    s.attn_shared()
     pump(2, 15)
     mem[1].came(1)
     mem[1].came(-1)
     pump(2, 16)
     mem[2].came(1)
     mem[2].came(-1)
+    attn[0].done()
     mem[0].done()
     mem[1].done()
+    mem[2].done()
     pump(2, 17)
+    s.attn_shared()
     s.out_first(0)
-    mem[2].done()
     s.out_first(1)
     s.mem_shared()
     s.out_last()

time: 82 us -> 78.7 us (0.960)
  Pallas kernels: 78.5 us -> 75.1 us
    pallas_call x1, Pallas kernels: 78.5 us -> 75.1 us  [shards(): pl.pallas_call(layer_kernel, out_shape=[pltpu.VMEM((HALF, 1024), bf), plt...]
where the time goes in v6:
time: 78.7 us; the launch traced here: 77.2 us
  Pallas kernels  75.1 us (95%)
  local copies, waits for them, and re-layouts  1.48 us (2%)
    pallas_call x1, Pallas kernels, shards(): pl.pallas_call(layer_kernel, out_shape=[pltpu.VMEM((HALF, 1024), bf), plt...  75.1 us

profile of v6, /device:TPU:0, one launch (start us, length us, event | category | flops | bytes accessed | tf_op | source)
XLA Modules:
  0.0 77.2 jit_solution(16498584694543146946)
XLA Ops:
  0.6 75.1 %layer.1 = (bf16[384,1024]{1,0:T(8,128)(2,1)S(1)}, f32[8,384]{1,0:T(8,128)S(1)}) custom-call(bf16[96,4096]{1,0:T(8,128)(2,1)} %tok.1, f32[1,4096]{1,0:T(1,128)} %bitcast.8, bf16[128,512]{1,0:T(8,128)(2,1)} %wq.1, bf16[128,128]{1,0:T(8,128)(2,1)} %wk.1, bf16[128,128]{1,0:T(8,128)(2,1)} %wv.1, bf16[128,256]{1,0:T(8,128)(2,1)} %wmq.1, bf16[128,256]{1,0:T(8,128)(2,1)} %wmk.1, ...), custom_call_target="tpu_custom_call" | custom-call | tf_op jit(solution)/shard_map/layer/pallas_call | solution.py:739
  75.7 0.9 %copy.18 = bf16[384,1024]{1,0:T(8,128)(2,1)} copy(bf16[384,1024]{1,0:T(8,128)(2,1)S(1)} %get-tuple-element.6) | data formatting | bytes 1572864
  76.6 0.6 copy.19

commit v7 on v6

--- a/solution.py
+++ b/solution.py
@@ -282,18 +282,24 @@
             kept[n] = fetch(half_of(c), block_rows(dst, c, depth, cols))
     gate_copy = fetch(wg, wgv)
 
+    pl.semaphore_wait(barrier, len(greeted))
+    sizes = (w1.at[0:128, 0:640], w2.at[0:128, :], w3.at[0:96, :])
+
+    def swap(n):
+        half_of, dst, depth, cols = pieces[n]
+        key = ("over", (n >= 4) + (n >= 6))
+        w.send(half_of(1 - c), block_rows(dst, c, depth, cols), w.partner(), "over", key)
+
+    for n in (0, 2, 3):
+        swap(n)
     k_copy.wait()
     v_copy.wait()
     kvp[0] = jnp.concatenate([rawkv[0, :, :HD], rawkv[1, :, :HD]], axis=1)
     kvp[1] = jnp.concatenate([rawkv[0, :, HD:], rawkv[1, :, HD:]], axis=1)
     sh[c] = fshift[...]
     kept[1] = fetch(kvp.at[c], block_rows(w1, c, 128, slice(256, 384)))
-    pl.semaphore_wait(barrier, len(greeted))
-
-    sizes = (w1.at[0:128, 0:640], w2.at[0:128, :], w3.at[0:96, :])
-    for n, (half_of, dst, depth, cols) in enumerate(pieces):
-        key = ("over", (n >= 4) + (n >= 6))
-        w.send(half_of(1 - c), block_rows(dst, c, depth, cols), w.partner(), "over", key)
+    for n in (1, 4, 5, 6):
+        swap(n)
 
     slots = {0: 0, -1: 1, 1: 2, 2: 3}
 
@@ -646,10 +652,11 @@
     s.tokens.start()
     pump(0, 8)
     s.gate_weights()
+    pump(0, 12)
+    s.tokens.came(1)
+    s.tokens.came(-1)
     pump(0, 14)
     pump(1, 4)
-    s.tokens.came(1)
-    s.tokens.came(-1)
     pump(0, 16)
     s.tokens.done()
     pump(1, 6)

time: 78.7 us -> 78.8 us (level)
  no operation moved by 1% of the time
where the time goes in v7:
time: 78.8 us; the launch traced here: 77.3 us
  Pallas kernels  75.2 us (95%)
  local copies, waits for them, and re-layouts  1.48 us (2%)
    pallas_call x1, Pallas kernels, shards(): pl.pallas_call(layer_kernel, out_shape=[pltpu.VMEM((HALF, 1024), bf), plt...  75.2 us

profile of v7, /device:TPU:0, one launch (start us, length us, event | category | flops | bytes accessed | tf_op | source)
XLA Modules:
  0.0 77.3 jit_solution(16661217746402467652)
XLA Ops:
  0.6 75.2 %layer.1 = (bf16[384,1024]{1,0:T(8,128)(2,1)S(1)}, f32[8,384]{1,0:T(8,128)S(1)}) custom-call(bf16[96,4096]{1,0:T(8,128)(2,1)} %tok.1, f32[1,4096]{1,0:T(1,128)} %bitcast.8, bf16[128,512]{1,0:T(8,128)(2,1)} %wq.1, bf16[128,128]{1,0:T(8,128)(2,1)} %wk.1, bf16[128,128]{1,0:T(8,128)(2,1)} %wv.1, bf16[128,256]{1,0:T(8,128)(2,1)} %wmq.1, bf16[128,256]{1,0:T(8,128)(2,1)} %wmk.1, ...), custom_call_target="tpu_custom_call" | custom-call | tf_op jit(solution)/shard_map/layer/pallas_call | solution.py:746
  75.8 0.9 %copy.18 = bf16[384,1024]{1,0:T(8,128)(2,1)} copy(bf16[384,1024]{1,0:T(8,128)(2,1)S(1)} %get-tuple-element.6) | data formatting | bytes 1572864
  76.7 0.6 copy.19
